TPU v7x, 256 devices: a whole 4x4x8 slice. The times are simulated.
256 devices in a mesh: sp: 32 (over z, x), tp: 8 (over y, core).
Axes of the slice: x: 4, y: 4, z: 8, core: 2. Of those that a mesh axis runs over, the one named last changes fastest.
Arguments:
- x_resid: bfloat16 [8192, 2048], P(('sp', 'tp')), may hold values from -3 to 3
- query_proj: bfloat16 [8192, 2048], P('sp', 'tp'), may hold values from -6 to 6
- projected_key_heads: bfloat16 [8192, 1024], P('sp', 'tp'), may hold values from -6 to 6
- projected_value_heads: bfloat16 [8192, 1024], P('sp', 'tp'), may hold values from -6 to 6
- query_gain: float32 [128], replicated, may hold values from 1.3 to 6.5
- key_norm_gain: float32 [128], replicated, may hold values from 1.3 to 6.5
- out_weight: bfloat16 [2048, 2048], P('tp'), may hold values from -0.125 to 0.125
- ffn_gain: float32 [2048], replicated, may hold values from 0.1 to 1.9
- routing: int32 [8192, 2], P(('sp', 'tp')), may hold values from 0 to 31, all different within a row; in each aligned block of 32 rows (0 to 31, 32 to 63, ...) at most 4 rows name the same one
- route_scores: float32 [8192, 2], P(('sp', 'tp')), may hold values from -6 to 6
- expert_gate: bfloat16 [32, 2048, 4096], P('sp', None, 'tp'), may hold values from -0.125 to 0.125
- expert_up: bfloat16 [32, 2048, 4096], P('sp', None, 'tp'), may hold values from -0.125 to 0.125
- expert_down: bfloat16 [32, 4096, 2048], P('sp', 'tp'), may hold values from -0.09375 to 0.09375
Outputs:
- layer_out: bfloat16 [8192, 2048], P(('sp', 'tp'))
Inputs may be any that keep to these rules, and one draw needn't show every extreme that they name: `routing`: each row names 2 different experts. In each aligned block of 32 rows (the rows of one device) no expert is named by more than 4 rows, a bound that some block reaches.
All inputs are finite; a program needn't handle non-finite values.
Results may differ from a plain program's by a relative error of at most 0.018.
The roundings to bfloat16 on the way count: a program that leaves them out, or rounds other values in their place, can miss the bound.
Values may be sent and summed in bfloat16 or wider, within the bound.
A program may use at most 128 MiB of HBM per device.

v0:
```python
import jax
import jax.numpy as jnp
from jax import lax
from jax.sharding import PartitionSpec as P

HEAD_WIDTH = 128
TOP = 2
GRID_W = 64


NORM_EPS = 1e-06
ROPE_BASE = 10000.0
NEG_LARGE = -1e30


def sent_together(arrays, axis, dim, along):
    widths = [a.shape[along] for a in arrays]
    both = jnp.concatenate(arrays, axis=along)
    whole = lax.all_gather(both, axis, axis=dim, tiled=True)
    return tuple(jnp.split(whole, [sum(widths[:k]) for k in range(1, len(widths))], axis=along))


def rms_scale(values, norm_gain):
    return (
        values * lax.rsqrt(jnp.mean(values * values, axis=-1, keepdims=True) + NORM_EPS) * norm_gain
    )


def grid_angles(token_positions, head_size):
    freq_count = head_size // 4
    frequency = ROPE_BASE ** (-jnp.arange(freq_count, dtype=jnp.float32) / freq_count)
    grid_row = (token_positions // GRID_W).astype(jnp.float32)
    grid_col = (token_positions % GRID_W).astype(jnp.float32)
    return (grid_row[:, None] * frequency, grid_col[:, None] * frequency)


def turn_half(values, angles):
    cosine = jnp.cos(angles)[:, None, :]
    sine_part = jnp.sin(angles)[:, None, :]
    leading, trailing = jnp.split(values, 2, axis=-1)
    return jnp.concatenate(
        [leading * cosine - trailing * sine_part, trailing * cosine + leading * sine_part], axis=-1
    )


def normalize_rotate(projected, norm_gain, token_positions, heads):
    length = projected.shape[0]
    values = projected.astype(jnp.float32).reshape(length, heads, -1)
    head_size = values.shape[-1]
    values = rms_scale(values, norm_gain)
    row_angle, col_angle = grid_angles(token_positions, head_size)
    half_size = head_size // 2
    turned = jnp.concatenate(
        [
            turn_half(values[..., :half_size], row_angle),
            turn_half(values[..., half_size:], col_angle),
        ],
        axis=-1,
    )
    return turned.reshape(length, heads * head_size).astype(jnp.bfloat16)


def local(
    x_resid,
    query_proj,
    projected_key_heads,
    projected_value_heads,
    query_gain,
    key_norm_gain,
    out_weight,
    ffn_gain,
    routing,
    route_scores,
    expert_gate,
    expert_up,
    expert_down,
):
    seq_rows = query_proj.shape[0]
    q_heads = query_proj.shape[1] // HEAD_WIDTH
    kv_heads = projected_key_heads.shape[1] // HEAD_WIDTH
    head_groups = q_heads // kv_heads
    token_positions = lax.axis_index("sp") * seq_rows + jnp.arange(seq_rows, dtype=jnp.int32)
    query_rows = normalize_rotate(query_proj, query_gain, token_positions, q_heads)
    rotated_key_rows = normalize_rotate(
        projected_key_heads, key_norm_gain, token_positions, kv_heads
    )
    query_grid = query_rows.reshape(seq_rows, kv_heads, head_groups, HEAD_WIDTH)
    score_scale = HEAD_WIDTH ** (-0.5)
    pieces = sent_together((rotated_key_rows, projected_value_heads), "sp", 0, 1)
    run_max = jnp.full((kv_heads, head_groups, seq_rows), NEG_LARGE, jnp.float32)
    key_piece = pieces[0].reshape(-1, kv_heads, HEAD_WIDTH)
    value_piece = pieces[1].reshape(-1, kv_heads, HEAD_WIDTH)
    scores = (
        jnp.einsum("qhgd,khd->hgqk", query_grid, key_piece, preferred_element_type=jnp.float32)
        * score_scale
    )
    new_max = jnp.maximum(run_max, jnp.max(scores, axis=-1))
    weights = jnp.exp(scores - new_max[..., None])
    new_total = jnp.sum(weights, axis=-1)
    addition = jnp.einsum(
        "hgqk,khd->hgqd",
        weights.astype(jnp.bfloat16),
        value_piece,
        preferred_element_type=jnp.float32,
    )
    attended = (
        (addition / new_total[..., None])
        .transpose(2, 0, 1, 3)
        .reshape(seq_rows, q_heads * HEAD_WIDTH)
        .astype(jnp.bfloat16)
    )
    own_tokens = x_resid.shape[0]
    model_width = x_resid.shape[1]
    row_block = attended
    attn_proj = lax.psum_scatter(
        jnp.dot(row_block, out_weight, preferred_element_type=jnp.float32).astype(jnp.bfloat16),
        "tp",
        scatter_dimension=0,
        tiled=True,
    )
    middle = x_resid.astype(jnp.float32) + attn_proj.astype(jnp.float32)
    normed = rms_scale(middle, ffn_gain).astype(jnp.bfloat16)
    experts_all = lax.axis_size("sp") * expert_gate.shape[0]
    capacity = max(2, 2 * own_tokens * TOP // experts_all)
    flat_expert = routing.reshape(-1)
    one_hot = (flat_expert[:, None] == jnp.arange(experts_all, dtype=jnp.int32)[None, :]).astype(
        jnp.int32
    )
    earlier = jnp.cumsum(one_hot, axis=0) - one_hot
    slot_rank = jnp.sum(earlier * one_hot, axis=1)
    target = flat_expert * capacity + slot_rank
    chooser = (
        jnp.arange(experts_all * capacity, dtype=jnp.int32)[:, None] == target[None, :]
    ).astype(jnp.float32)
    gate_share = jax.nn.softmax(route_scores, axis=-1).reshape(-1)
    picker = jnp.sum(chooser.reshape(experts_all * capacity, own_tokens, TOP), axis=2).astype(
        jnp.bfloat16
    )
    combiner = jnp.sum(
        (chooser * gate_share[None, :]).reshape(experts_all * capacity, own_tokens, TOP), axis=2
    )
    dispatch = (
        jnp.dot(picker, normed, preferred_element_type=jnp.float32)
        .astype(jnp.bfloat16)
        .reshape(experts_all, capacity, model_width)
    )
    gate_matrix = expert_gate[0]
    up_matrix = expert_up[0]
    down_matrix = expert_down[0]
    arrived = lax.all_to_all(dispatch, "sp", split_axis=0, concat_axis=0, tiled=True)
    row_block = lax.all_gather(arrived.reshape(-1, model_width), "tp", axis=0, tiled=True)
    gate_part = jnp.dot(row_block, gate_matrix, preferred_element_type=jnp.float32)
    up_part = jnp.dot(row_block, up_matrix, preferred_element_type=jnp.float32)
    hidden = (jax.nn.silu(gate_part) * up_part).astype(jnp.bfloat16)
    row_block = hidden
    expert_result = lax.psum_scatter(
        jnp.dot(row_block, down_matrix, preferred_element_type=jnp.float32).astype(jnp.bfloat16),
        "tp",
        scatter_dimension=0,
        tiled=True,
    )
    returned = lax.all_to_all(
        expert_result.reshape(-1, capacity, model_width),
        "sp",
        split_axis=0,
        concat_axis=0,
        tiled=True,
    )
    routed = jnp.einsum(
        "st,sd->td", combiner, returned.reshape(-1, model_width).astype(jnp.float32)
    )
    return (middle + routed).astype(jnp.bfloat16)


def solution(mesh):
    in_specs = (
        P(("sp", "tp"), None),
        P("sp", "tp"),
        P("sp", "tp"),
        P("sp", "tp"),
        P(),
        P(),
        P("tp", None),
        P(),
        P(("sp", "tp"), None),
        P(("sp", "tp"), None),
        P("sp", None, "tp"),
        P("sp", None, "tp"),
        P("sp", "tp", None),
    )
    out_specs = P(("sp", "tp"), None)
    return jax.shard_map(local, mesh=mesh, in_specs=in_specs, out_specs=out_specs, check_vma=False)
```

profile of v0, /device:TPU:0, one launch (start us, length us, event | category | flops | bytes accessed | tf_op | source)
XLA Modules:
  0.0 308.2 jit_solution(1226944884307832403)
XLA Ops:
  6.6 1.1 copy.36
  7.7 0.9 copy.37
  8.7 0.7 fusion.25
  9.4 0.3 fusion.48
  9.7 0.7 pad_maximum_fusion
  10.4 0.0 all-gather.3.cloned.1.call-update
  10.4 0.0 reduce-scatter.3.cloned.1.call-start
  10.5 1.0 copy.38
  11.5 0.1 copy.39
  11.7 1.0 multiply_cosine_fusion.1
  12.7 0.8 multiply_multiply_fusion
  13.4 0.3 subtract_convert_fusion.1
  13.7 80.7 %all-gather.3.cloned.1.call-done = bf16[8192,256]{0,1:T(8,128)(2,1)} async-done(((bf16[256,256]{0,1:T(8,128)(2,1)}), bf16[8192,256]{0,1:T(8,128)(2,1)}) %all-gather.3.cloned.1.call-update) | async-done | bytes 4194320 | tf_op jit(solution)/shard_map/all_gather | solution.py:19
  94.4 9.8 %bitcast_reduce_fusion = (f32[2,256]{1,0:T(2,128)S(1)}, f32[8192,256,2]{1,0,2:T(8,128)}) fusion(bf16[256,2,32]{2,0,1:T(8,128)(2,1)S(1)} %get-tuple-element.11, bf16[256,2,32]{2,0,1:T(8,128)(2,1)S(1)} %get-tuple-element.12, bf16[256,2,32]{2,0,1:T(8,128)(2,1)S(1)} %get-tuple-element.8, bf16[256,2,32]{2,0,1:T(8,128)(2,1)S(1)} %get-tuple-element.7, ...), kind=kOutput, calls=%fused_computation.1 | convolution fusion | flops 1082654208 | bytes 19007488 | tf_op jit(solution)/shard_map/qhgd,khd->hgqk/dot_general | solution.py:94
  104.3 8.7 %fusion.1 = f32[2,256]{1,0:T(2,128)S(1)} fusion(f32[8192,256,2]{1,0,2:T(8,128)} %get-tuple-element.26, f32[2,256]{1,0:T(2,128)S(1)} %broadcast_maximum_fusion), kind=kLoop, calls=%fused_computation.3 | loop fusion | flops 12582400 | bytes 16781312 | tf_op jit(solution)/shard_map/reduce_sum | solution.py:99
  112.9 0.0 copy-start.4
  112.9 0.0 copy-start.7
  113.0 0.0 copy-start.2
  113.0 0.0 copy-start.6
  113.0 7.5 %fusion.18 = bf16[2,256,128]{1,2,0:T(8,128)(2,1)S(1)} fusion(f32[8192,256,2]{1,0,2:T(8,128)} %get-tuple-element.26, f32[2,256]{1,0:T(2,128)S(1)} %broadcast_maximum_fusion, bf16[8192,256]{0,1:T(8,128)(2,1)S(1)} %copy-done.1, f32[2,256]{1,0:T(2,128)S(1)} %fusion.1), kind=kOutput, calls=%fused_computation.22 | convolution fusion | flops 1086455808 | bytes 19009536 | tf_op jit(solution)/shard_map/hgqk,khd->hgqd/dot_general | solution.py:100
  120.5 1.5 convolution_convert_fusion.1
  121.9 0.0 reduce-scatter.3.cloned.1.call-update
  121.9 0.0 all-gather.5.cloned.1.call-start
  122.0 0.1 copy.42
  122.1 0.1 eq.34
  122.2 0.1 fusion.51
  122.3 0.1 reduce_window_sum.11
  122.4 0.2 select_reduce_fusion.1
  122.6 0.1 reduce_sum.78
  122.7 0.1 copy.43
  122.8 0.1 convert_reduce_fusion
  122.9 34.6 %reduce-scatter.3.cloned.1.call-done = bf16[32,2048]{1,0:T(8,128)(2,1)} async-done(((bf16[256,2048]{1,0:T(8,128)(2,1)}), bf16[32,2048]{1,0:T(8,128)(2,1)}) %reduce-scatter.3.cloned.1.call-update) | async-done | bytes 131088 | tf_op jit(solution)/shard_map/reduce_scatter | solution.py:115
  157.6 1.1 multiply_reduce_fusion
  158.6 1.3 convolution_convert_fusion.2
  159.9 0.2 reshape.358
  160.1 25.1 %all_to_all.10 = bf16[32,4,2048]{2,1,0:T(4,128)(2,1)S(1)} all-to-all(bf16[32,4,2048]{2,1,0:T(4,128)(2,1)S(1)} %reshape.358), channel_id=1, replica_groups=mesh['sp'=32,'tp'=8] {'sp'}, dimensions={0} | all-to-all | bytes 1048576 | tf_op jit(solution)/shard_map/all_to_all | solution.py:150
  185.2 0.9 reshape.359
  186.1 0.0 all-gather.5.cloned.1.call-update
  186.2 0.2 reduce-scatter.5.cloned.1.call-start
  186.4 31.0 %all-gather.5.cloned.1.call-done = bf16[1024,2048]{1,0:T(8,128)(2,1)} async-done(((bf16[128,2048]{1,0:T(8,128)(2,1)}), bf16[1024,2048]{1,0:T(8,128)(2,1)}) %all-gather.5.cloned.1.call-update) | async-done | bytes 4194320 | tf_op jit(solution)/shard_map/all_gather | solution.py:151
  217.3 6.6 %fusion.9 = f32[1024,512]{1,0:T(8,128)} fusion(bf16[1024,2048]{1,0:T(8,128)(2,1)} %all-gather.5.cloned.1.call-done, bf16[1,2048,512]{2,1,0:T(8,128)(2,1)} %param.24), kind=kOutput, calls=%fused_computation.16 | convolution fusion | flops 2147483648 | bytes 8388608 | tf_op jit(solution)/shard_map/dot_general | solution.py:153
  223.9 10.1 %convolution_convert_fusion = bf16[1024,2048]{1,0:T(8,128)(2,1)} fusion(bf16[1,512,2048]{2,1,0:T(8,128)(2,1)S(1)} %copy-done, f32[1024,512]{1,0:T(8,128)} %fusion.9, bf16[1024,2048]{1,0:T(8,128)(2,1)} %all-gather.5.cloned.1.call-done, bf16[1,2048,512]{2,1,0:T(8,128)(2,1)} %param.23), kind=kOutput, calls=%fused_computation.7 | convolution fusion | flops 4300210176 | bytes 14680064 | tf_op jit(solution)/shard_map/dot_general | solution.py:157
  234.0 0.0 reduce-scatter.5.cloned.1.call-update
  234.1 40.7 %reduce-scatter.5.cloned.1.call-done = bf16[128,2048]{1,0:T(8,128)(2,1)} async-done(((bf16[1024,2048]{1,0:T(8,128)(2,1)}), bf16[128,2048]{1,0:T(8,128)(2,1)}) %reduce-scatter.5.cloned.1.call-update) | async-done | bytes 524304 | tf_op jit(solution)/shard_map/reduce_scatter | solution.py:156
  274.7 1.2 reshape.360
  275.9 24.7 %all_to_all.11 = bf16[32,4,2048]{2,1,0:T(4,128)(2,1)S(1)} all-to-all(bf16[32,4,2048]{2,1,0:T(4,128)(2,1)S(1)} %reshape.360), channel_id=1, replica_groups=mesh['sp'=32,'tp'=8] {'sp'}, dimensions={0} | all-to-all | bytes 1048576 | tf_op jit(solution)/shard_map/all_to_all | solution.py:162
  300.7 0.1 reshape.361
  300.8 0.9 fusion.6
  (26 shorter events, 0.2 us)
Async XLA Ops:
  6.5 217.4 %copy-start = (bf16[1,512,2048]{2,1,0:T(8,128)(2,1)S(1)}, bf16[1,512,2048]{2,1,0:T(8,128)(2,1)}, u32[]{:S(2)}) copy-start(bf16[1,512,2048]{2,1,0:T(8,128)(2,1)} %param.25) | copy-start | bytes 6291460
  6.5 87.9 %all-gather.3.cloned.1.call-start = ((), (), s32[]{:S(2)}) async-start(), calls=%async_computation.4 | async-start | bytes 4325376 | tf_op jit(solution)/shard_map/all_gather | solution.py:19
  10.4 147.1 %reduce-scatter.3.cloned.1.call-start = ((), (), s32[]{:S(2)}) async-start(), calls=%async_computation.5 | async-start | bytes 1179648 | tf_op jit(solution)/shard_map/reduce_scatter | solution.py:115
  104.3 8.7 %copy-start.1 = (bf16[8192,256]{0,1:T(8,128)(2,1)S(1)}, bf16[8192,256]{0,1:T(8,128)(2,1)}, u32[]{:S(2)}) copy-start(bf16[8192,256]{0,1:T(8,128)(2,1)} %all-gather.3.cloned.1.call-done) | copy-start | bytes 12582916
  112.9 7.5 %copy-start.4 = (bf16[256,2048]{1,0:T(8,128)(2,1)S(1)}, bf16[256,2048]{1,0:T(8,128)(2,1)}, u32[]{:S(2)}) copy-start(bf16[256,2048]{1,0:T(8,128)(2,1)} %param.19) | copy-start | bytes 3145732
  112.9 9.1 %copy-start.7 = (s32[32,2]{0,1:T(2,128)S(1)}, s32[32,2]{0,1:T(2,128)}, u32[]{:S(2)}) copy-start(s32[32,2]{0,1:T(2,128)} %param.21) | copy-start | bytes 772
  112.9 9.8 %copy-start.5 = (f32[32,2]{0,1:T(2,128)S(1)}, f32[32,2]{0,1:T(2,128)}, u32[]{:S(2)}) copy-start(f32[32,2]{0,1:T(2,128)} %param.22) | copy-start | bytes 772
  113.0 44.6 %copy-start.2 = (bf16[32,2048]{1,0:T(8,128)(2,1)S(1)}, bf16[32,2048]{1,0:T(8,128)(2,1)}, u32[]{:S(2)}) copy-start(bf16[32,2048]{1,0:T(8,128)(2,1)} %param.13) | copy-start | bytes 393220
  113.0 45.6 %copy-start.6 = (f32[2048]{0:T(1024)S(1)}, f32[2048]{0:T(1024)}, u32[]{:S(2)}) copy-start(f32[2048]{0:T(1024)} %param.20) | copy-start | bytes 24580
  121.9 95.4 %all-gather.5.cloned.1.call-start = ((), (), s32[]{:S(2)}) async-start(), calls=%async_computation.6 | async-start | bytes 4718592 | tf_op jit(solution)/shard_map/all_gather | solution.py:151
  186.2 88.5 %reduce-scatter.5.cloned.1.call-start = ((), (), s32[]{:S(2)}) async-start(), calls=%async_computation.7 | async-start | bytes 4718592 | tf_op jit(solution)/shard_map/reduce_scatter | solution.py:156
  234.0 66.8 %copy-start.3 = (bf16[32,2048]{1,0:T(8,128)(2,1)S(1)}, bf16[32,2048]{1,0:T(8,128)(2,1)}, u32[]{:S(2)}) copy-start(bf16[32,2048]{1,0:T(8,128)(2,1)} %reduce-scatter.3.cloned.1.call-done) | copy-start | bytes 393220
Sparse Core Ops, SparseCore 0:
  10.6 83.8 all-gather.2
  122.1 35.4 reduce-scatter.2
  186.3 31.0 all-gather.4
  234.2 40.4 reduce-scatter.4
where the time goes:
time: 310 us; the launch traced here: 308 us
  waiting for transfers between devices  187 us (60%)
  blocking collectives  49.9 us (16%)
  matrix products  37.5 us (12%)
  other arithmetic  14.1 us (5%)
  between operations  13.4 us (4%)
  local copies, waits for them, and re-layouts  6.01 us (2%)
    all_gather x1, waiting for transfers between devices, sent_together(): whole = lax.all_gather(both, axis, axis=dim, tiled=True)  80.7 us
    reduce_scatter x1, waiting for transfers between devices, local(): lax.psum_scatter(jnp.dot(row_block, down_matrix, preferred_element_type=j...  40.7 us
    reduce_scatter x1, waiting for transfers between devices, local(): lax.psum_scatter(jnp.dot(row_block, out_weight, preferred_element_type=jn...  34.6 us
    all_gather x1, waiting for transfers between devices, local(): lax.all_gather(arrived.reshape(-1, model_width), 'tp', axis=0, tiled=True)  31 us
    all_to_all x1, blocking collectives, local(): lax.all_to_all(dispatch, 'sp', split_axis=0, concat_axis=0, tiled=True)  25.1 us
    all_to_all x1, blocking collectives, local(): lax.all_to_all(expert_result.reshape(-1, capacity, model_width), 'sp', sp...  24.7 us
    dot_general x1, matrix products, local(): jnp.dot(row_block, down_matrix, preferred_element_type=jnp.float32)  10.1 us
    dot_general x1, matrix products, local(): jnp.einsum('qhgd,khd->hgqk', query_grid, key_piece, preferred_element_typ...  9.81 us
  transfers between devices with their start and end apart: 4, of which 4 were waited for; matrix products, arithmetic and copies ran while one was open for 1% of the time, Pallas kernels for 0%

commit v1 on v0

v1 whole, which is shorter than its diff:
```python
import functools
import jax
import jax.numpy as jnp
from jax import lax
from jax.experimental import pallas as pl
from jax.experimental.pallas import tpu as pltpu
from jax.sharding import PartitionSpec as P

HEAD_WIDTH = 128
TOP = 2
GRID_W = 64
NORM_EPS = 1e-06
ROPE_BASE = 10000.0
NEG_LARGE = -1e30
LOG2E = 1.4426950408889634
MESH = pl.DeviceIdType.MESH

NZ, NX, NY = 8, 4, 4
N_SP = NZ * NX
N_TP = NY * 2
SEQ = 256
ROWS_A = 96
ARRIVALS = [('A', 0, 1), ('A', 0, -1), ('B', 1, 0), ('B', -1, 0), ('B', 0, -1), ('A', 1, 0), ('A', -1, 0), ('A', 0, 2), ('A', 1, 1), ('A', -1, 1), ('B', 0, 1), ('A', 1, -1), ('A', -1, -1), ('B', 1, -1), ('B', 1, 1), ('B', 2, 0), ('B', -2, 0), ('B', -1, -1), ('A', 2, 0), ('A', -2, 0), ('B', -1, 1), ('A', 1, 2), ('A', -1, 2), ('B', 1, 2), ('A', 2, 1), ('A', -2, 1), ('B', 0, 2), ('B', 2, -1), ('A', 2, -1), ('A', -2, -1), ('B', 2, 1), ('B', -2, -1), ('B', 3, 0), ('B', -3, 0), ('B', -2, 1), ('A', 3, 0), ('A', -3, 0), ('B', -1, 2), ('A', 2, 2), ('A', -2, 2), ('B', 2, 2), ('A', 3, 1), ('A', -3, 1), ('B', 3, -1), ('A', 3, -1), ('A', -3, -1), ('B', 3, 1), ('A', -3, 2), ('B', -3, -1), ('B', 4, 0), ('B', -3, 1), ('A', 4, 0), ('A', 4, -1), ('B', 3, 2), ('B', -2, 2), ('A', 3, 2), ('A', 4, 2), ('A', 4, 1), ('B', -3, 2), ('B', 4, 1), ('B', 4, -1), ('B', 4, 2)]


def rms_scale(values, norm_gain):
    return (
        values * lax.rsqrt(jnp.mean(values * values, axis=-1, keepdims=True) + NORM_EPS) * norm_gain
    )


def turn_tables(token_positions):
    freq_count = HEAD_WIDTH // 4
    frequency = ROPE_BASE ** (-jnp.arange(freq_count, dtype=jnp.float32) / freq_count)
    row = (token_positions // GRID_W).astype(jnp.float32)[:, None] * frequency
    col = (token_positions % GRID_W).astype(jnp.float32)[:, None] * frequency
    angles = jnp.concatenate([row, row, col, col], axis=-1)
    sign = jnp.where((jnp.arange(HEAD_WIDTH) // freq_count) % 2 == 0, -1.0, 1.0)
    return jnp.cos(angles), jnp.sin(angles) * sign.astype(jnp.float32)


def turned(values, gain, cos, sin):
    normed = rms_scale(values, gain)
    lane = lax.broadcasted_iota(jnp.int32, normed.shape, 1)
    partner = jnp.where(
        lane % 64 < 32, pltpu.roll(normed, 96, 1), pltpu.roll(normed, 32, 1)
    )
    return (normed * cos + partner * sin).astype(jnp.bfloat16)


def attention_kernel(
    q_ref, k_ref, v_ref, qg_ref, kg_ref, cos_ref, sin_ref, w_ref, x_ref, fg_ref,
    mid_ref, normed_ref,
    kv, qs, m_ref, l_ref, acc, wfull, att, att_in,
    send_sem, recv_a, recv_b, recv_w, recv_att, own_sem,
):
    sp = lax.axis_index("sp")
    tp = lax.axis_index("tp")
    z, x = sp // NX, sp % NX
    y, c = tp // 2, tp % 2

    def sp_of(dz, dx):
        return ((z - dz + 2 * NZ) % NZ) * NX + (x - dx + 2 * NX) % NX

    def tp_of(dy, other=False):
        return ((y + dy + NY) % NY) * 2 + ((1 - c) if other else c)

    own_w = pltpu.make_async_copy(w_ref, wfull.at[tp], own_sem)
    own_w.start()

    barrier = pltpu.get_barrier_semaphore()
    friends = [(sp_of(dz, dx), tp) for dz, dx in ((1, 0), (-1, 0), (0, 1), (0, -1), (0, 2))]
    friends += [(sp, tp_of(dy, o)) for dy in range(NY) for o in (False, True) if (dy, o) != (0, False)]
    for dev in friends:
        pl.semaphore_signal(barrier, inc=1, device_id=dev, device_id_type=MESH)

    cos, sin = cos_ref[...], sin_ref[...]
    kv[sp, :, 0:128] = turned(k_ref[...].astype(jnp.float32), kg_ref[...], cos, sin)
    kv[sp, :, 128:256] = v_ref[...]
    for h in range(2):
        qs[h] = turned(
            q_ref[:, h * 128 : (h + 1) * 128].astype(jnp.float32), qg_ref[...], cos, sin
        )
    m_ref[...] = jnp.full(m_ref.shape, NEG_LARGE, jnp.float32)
    l_ref[...] = jnp.zeros(l_ref.shape, jnp.float32)
    acc[...] = jnp.zeros(acc.shape, jnp.float32)
    pl.semaphore_wait(barrier, len(friends))

    sent = []

    def send(src, dst, recv, dev):
        copy = pltpu.make_async_remote_copy(
            src_ref=src, dst_ref=dst, send_sem=send_sem.at[len(sent)], recv_sem=recv,
            device_id=dev, device_id_type=MESH,
        )
        copy.start()
        sent.append(copy)

    def arrived(ref, recv):
        pltpu.make_async_remote_copy(
            src_ref=ref, dst_ref=ref, send_sem=send_sem.at[0], recv_sem=recv,
            device_id=(sp, tp_of(0, True)), device_id_type=MESH,
        ).wait_recv()

    def piece(half, owner):
        if half == "A":
            return kv.at[owner, pl.ds(0, ROWS_A)], recv_a.at[owner]
        return kv.at[owner, pl.ds(ROWS_A, SEQ - ROWS_A)], recv_b.at[owner]

    def pass_on(half, dz, dx, link):
        ref, recv = piece(half, sp_of(dz, dx))
        dev = {
            "z+": (sp_of(-1, 0), tp), "z-": (sp_of(1, 0), tp),
            "x+": (sp_of(0, -1), tp), "x-": (sp_of(0, 1), tp), "x2": (sp_of(0, 2), tp),
        }[link]
        send(ref, ref, recv, dev)

    def next_links(half, dz, dx):
        if half == "A":
            if dz == 0:
                return ["z+", "z-"]
            if dz in (1, 2) or (dz == 3 and dx in (0, 1)):
                return ["z+"]
            if dz in (-1, -2) or (dz == -3 and dx in (-1, 2)):
                return ["z-"]
            return []
        if dx == 0:
            along = ["z+"] if dz in (1, 2, 3) else ["z-"] if dz in (-1, -2) else []
            return along + ["x+", "x-"]
        if dx == 1 and dz % 2 == 0:
            return ["x+"]
        if dx == -1 and dz % 2 == 1:
            return ["x-"]
        return []

    def w_half(owner, half):
        return wfull.at[owner, pl.ds(half * 128, 128)], recv_w.at[owner, half]

    for half, dz, dx, link in (
        ("B", 0, 0, "z+"), ("B", 0, 0, "z-"), ("A", 0, 0, "x+"), ("A", 0, 0, "x-"),
        ("A", 0, 0, "x2"), ("B", 0, 0, "x+"), ("B", 0, 0, "x-"), ("A", 0, 0, "z+"),
        ("A", 0, 0, "z-"),
    ):
        pass_on(half, dz, dx, link)
    for half, dev in ((0, tp_of(1)), (1, tp_of(-1)), (1, tp_of(1)), (0, tp_of(-1))):
        dst, recv = w_half(tp, half)
        send(w_ref.at[pl.ds(half * 128, 128)], dst, recv, (sp, dev))
    for half in (0, 1):
        dst, recv = w_half(tp, half)
        send(w_ref.at[pl.ds(half * 128, 128)], dst, recv, (sp, tp_of(0, True)))

    def w_event(dy, half, links):
        ref, recv = w_half(tp_of(dy), half)
        arrived(ref, recv)
        for link in links:
            dev = tp_of(0, True) if link == 0 else tp_of(link)
            send(ref, ref, recv, (sp, dev))

    scale2 = HEAD_WIDTH ** (-0.5) * LOG2E

    def attend(group):
        def step(i, carry):
            block = kv[pl.ds(group * NX + 2 * i, 2)].reshape(2 * SEQ, 256)
            keys, values = block[:, 0:128], block[:, 128:256]
            for h in range(2):
                s = lax.dot_general(
                    qs[h], keys, (((1,), (1,)), ((), ())), preferred_element_type=jnp.float32
                )
                m_old = m_ref[h]
                m_new = jnp.maximum(m_old, jnp.max(s, axis=1, keepdims=True))
                alpha = jnp.exp2((m_old - m_new) * scale2)
                m_all = jnp.concatenate([m_new * scale2] * 4, axis=1)
                p = jnp.exp2(s * scale2 - m_all)
                l_ref[h] = l_ref[h] * alpha + (
                    (p[:, 0:128] + p[:, 128:256]) + (p[:, 256:384] + p[:, 384:512])
                )
                acc[h] = acc[h] * alpha + jnp.dot(
                    p.astype(jnp.bfloat16), values, preferred_element_type=jnp.float32
                )
                m_ref[h] = m_new
            return carry

        lax.fori_loop(0, NX // 2, step, 0)

    left = {dz: (6 if dz == 0 else 8) for dz in (0, 1, -1, 2, -2, 3, -3, 4)}
    w_plan = {24: ((-1, 0, (1, 0)), (1, 1, (-1, 0))), 55: ((-1, 1, (0,)), (1, 0, (0,)))}
    ready = []
    for count, (half, dz, dx) in enumerate(ARRIVALS):
        ref, recv = piece(half, sp_of(dz, dx))
        arrived(ref, recv)
        for link in next_links(half, dz, dx):
            pass_on(half, dz, dx, link)
        for dy, w_part, links in w_plan.get(count, ()):
            w_event(dy, w_part, links)
        left[dz] -= 1
        if left[dz] == 0:
            attend((z - dz + NZ) % NZ)

    for h in range(2):
        total = jnp.sum(l_ref[h], axis=1, keepdims=True)
        att[:, h * 128 : (h + 1) * 128] = (acc[h] / total).astype(jnp.bfloat16)

    att_in[tp] = att[pl.ds(tp * 32, 32), :]
    for dy, other in ((0, True), (1, False), (1, True), (3, False), (3, True), (2, False), (2, True)):
        to = tp_of(dy, other)
        send(att.at[pl.ds(to * 32, 32)], att_in.at[tp], recv_att.at[tp], (sp, to))

    own_w.wait()
    w_event(2, 0, (0,))
    w_event(2, 1, (0,))
    total = jnp.zeros((32, 2048), jnp.float32)
    order = [(0, False), (0, True), (1, False), (3, False), (1, True), (3, True), (2, False), (2, True)]
    for dy, other in order:
        owner = tp_of(dy, other)
        if (dy, other) != (0, False):
            arrived(att_in.at[owner], recv_att.at[owner])
        if other:
            for half in (0, 1):
                ref, recv = w_half(owner, half)
                arrived(ref, recv)
        part = jnp.dot(att_in[owner], wfull[owner], preferred_element_type=jnp.float32)
        total = total + part.astype(jnp.bfloat16).astype(jnp.float32)
    middle = x_ref[...].astype(jnp.float32) + total.astype(jnp.bfloat16).astype(jnp.float32)
    mid_ref[...] = middle
    normed_ref[...] = rms_scale(middle, fg_ref[...]).astype(jnp.bfloat16)
    for copy in sent:
        copy.wait_send()


def attention_part(x_resid, query_proj, keys, values, query_gain, key_gain, out_weight, ffn_gain):
    positions = lax.axis_index("sp") * SEQ + jnp.arange(SEQ, dtype=jnp.int32)
    cos, sin = turn_tables(positions)
    vmem = pl.BlockSpec(memory_space=pltpu.VMEM)
    return pl.pallas_call(
        attention_kernel,
        out_shape=(
            jax.ShapeDtypeStruct((32, 2048), jnp.float32),
            jax.ShapeDtypeStruct((32, 2048), jnp.bfloat16),
        ),
        in_specs=[vmem] * 7 + [pl.BlockSpec(memory_space=pl.ANY)] + [vmem] * 2,
        out_specs=(vmem, vmem),
        scratch_shapes=[
            pltpu.VMEM((N_SP, SEQ, 256), jnp.bfloat16),
            pltpu.VMEM((2, SEQ, 128), jnp.bfloat16),
            pltpu.VMEM((2, SEQ, 128), jnp.float32),
            pltpu.VMEM((2, SEQ, 128), jnp.float32),
            pltpu.VMEM((2, SEQ, 128), jnp.float32),
            pltpu.VMEM((N_TP, 256, 2048), jnp.bfloat16),
            pltpu.VMEM((SEQ, 256), jnp.bfloat16),
            pltpu.VMEM((N_TP, 32, 256), jnp.bfloat16),
            pltpu.SemaphoreType.DMA((96,)),
            pltpu.SemaphoreType.DMA((N_SP,)),
            pltpu.SemaphoreType.DMA((N_SP,)),
            pltpu.SemaphoreType.DMA((N_TP, 2)),
            pltpu.SemaphoreType.DMA((N_TP,)),
            pltpu.SemaphoreType.DMA,
        ],
        compiler_params=pltpu.CompilerParams(
            collective_id=0, has_side_effects=True, vmem_limit_bytes=40 * 1024 * 1024
        ),
        name="attention",
    )(
        query_proj, keys, values, query_gain.reshape(1, -1), key_gain.reshape(1, -1), cos, sin,
        out_weight, x_resid, ffn_gain.reshape(1, -1),
    )


def local(
    x_resid,
    query_proj,
    projected_key_heads,
    projected_value_heads,
    query_gain,
    key_norm_gain,
    out_weight,
    ffn_gain,
    routing,
    route_scores,
    expert_gate,
    expert_up,
    expert_down,
):
    own_tokens = x_resid.shape[0]
    model_width = x_resid.shape[1]
    middle, normed = attention_part(
        x_resid, query_proj, projected_key_heads, projected_value_heads, query_gain,
        key_norm_gain, out_weight, ffn_gain,
    )
    experts_all = lax.axis_size("sp") * expert_gate.shape[0]
    capacity = max(2, 2 * own_tokens * TOP // experts_all)
    flat_expert = routing.reshape(-1)
    one_hot = (flat_expert[:, None] == jnp.arange(experts_all, dtype=jnp.int32)[None, :]).astype(
        jnp.int32
    )
    earlier = jnp.cumsum(one_hot, axis=0) - one_hot
    slot_rank = jnp.sum(earlier * one_hot, axis=1)
    target = flat_expert * capacity + slot_rank
    chooser = (
        jnp.arange(experts_all * capacity, dtype=jnp.int32)[:, None] == target[None, :]
    ).astype(jnp.float32)
    gate_share = jax.nn.softmax(route_scores, axis=-1).reshape(-1)
    picker = jnp.sum(chooser.reshape(experts_all * capacity, own_tokens, TOP), axis=2).astype(
        jnp.bfloat16
    )
    combiner = jnp.sum(
        (chooser * gate_share[None, :]).reshape(experts_all * capacity, own_tokens, TOP), axis=2
    )
    dispatch = (
        jnp.dot(picker, normed, preferred_element_type=jnp.float32)
        .astype(jnp.bfloat16)
        .reshape(experts_all, capacity, model_width)
    )
    gate_matrix = expert_gate[0]
    up_matrix = expert_up[0]
    down_matrix = expert_down[0]
    arrived = lax.all_to_all(dispatch, "sp", split_axis=0, concat_axis=0, tiled=True)
    row_block = lax.all_gather(arrived.reshape(-1, model_width), "tp", axis=0, tiled=True)
    gate_part = jnp.dot(row_block, gate_matrix, preferred_element_type=jnp.float32)
    up_part = jnp.dot(row_block, up_matrix, preferred_element_type=jnp.float32)
    hidden = (jax.nn.silu(gate_part) * up_part).astype(jnp.bfloat16)
    row_block = hidden
    expert_result = lax.psum_scatter(
        jnp.dot(row_block, down_matrix, preferred_element_type=jnp.float32).astype(jnp.bfloat16),
        "tp",
        scatter_dimension=0,
        tiled=True,
    )
    returned = lax.all_to_all(
        expert_result.reshape(-1, capacity, model_width),
        "sp",
        split_axis=0,
        concat_axis=0,
        tiled=True,
    )
    routed = jnp.einsum(
        "st,sd->td", combiner, returned.reshape(-1, model_width).astype(jnp.float32)
    )
    return (middle + routed).astype(jnp.bfloat16)


def solution(mesh):
    in_specs = (
        P(("sp", "tp"), None),
        P("sp", "tp"),
        P("sp", "tp"),
        P("sp", "tp"),
        P(),
        P(),
        P("tp", None),
        P(),
        P(("sp", "tp"), None),
        P(("sp", "tp"), None),
        P("sp", None, "tp"),
        P("sp", None, "tp"),
        P("sp", "tp", None),
    )
    out_specs = P(("sp", "tp"), None)
    return jax.shard_map(local, mesh=mesh, in_specs=in_specs, out_specs=out_specs, check_vma=False)
```

time: 310 us -> 217 us (0.70)
  waiting for transfers between devices: 187 us -> 70.2 us
  Pallas kernels: 0 us -> 51.4 us
  matrix products: 37.5 us -> 17.9 us
  other arithmetic: 14.1 us -> 4.08 us
  local copies, waits for them, and re-layouts: 6.01 us -> 10.2 us
    all_gather x1 -> x0, waiting for transfers between devices: 80.7 us -> none  [sent_together(): whole = lax.all_gather(both, axis, axis=dim, tiled=True)]
    pallas_call x0 -> x1, Pallas kernels: none -> 51.4 us  [attention_part(): pl.pallas_call(attention_kernel, out_shape=(jax.ShapeDtypeStruct((32, 204...]
    reduce_scatter x1 -> x0, waiting for transfers between devices: 34.6 us -> none  [local(): lax.psum_scatter(jnp.dot(row_block, out_weight, preferred_element_type=jn...]
    dot_general x3 -> x0, matrix products: 18.7 us -> none  [the longest x1 9.81 us: local(): jnp.einsum('qhgd,khd->hgqk', query_grid, key_piece, preferred_element_typ...]
    reduce_sum x4 -> x0, other arithmetic: 9.79 us -> none  [the longest x1 8.65 us: local(): new_total = jnp.sum(weights, axis=-1)]
    unnamed x20 -> x19, local copies, waits for them, and re-layouts: 3.16 us -> 7.48 us
  transfers between devices with their start and end apart: 4 -> 2, of which waited for: 4 -> 2; matrix products, arithmetic and copies ran while one was open for 1% -> 0% of each run, Pallas kernels for 0% -> 0%
where the time goes in v1:
time: 217 us; the launch traced here: 215 us
  waiting for transfers between devices  70.2 us (32%)
  Pallas kernels  51.4 us (24%)
  blocking collectives  47.5 us (22%)
  matrix products  17.9 us (8%)
  between operations  13.5 us (6%)
  local copies, waits for them, and re-layouts  10.2 us (5%)
  other arithmetic  4.08 us (2%)
    pallas_call x1, Pallas kernels, attention_part(): pl.pallas_call(attention_kernel, out_shape=(jax.ShapeDtypeStruct((32, 204...  51.4 us
    reduce_scatter x1, waiting for transfers between devices, local(): lax.psum_scatter(jnp.dot(row_block, down_matrix, preferred_element_type=j...  40.6 us
    all_gather x1, waiting for transfers between devices, local(): lax.all_gather(arrived.reshape(-1, model_width), 'tp', axis=0, tiled=True)  29.5 us
    all_to_all x1, blocking collectives, local(): lax.all_to_all(expert_result.reshape(-1, capacity, model_width), 'sp', sp...  24.8 us
    all_to_all x1, blocking collectives, local(): lax.all_to_all(dispatch, 'sp', split_axis=0, concat_axis=0, tiled=True)  22.7 us
    dot_general x1, matrix products, local(): jnp.dot(row_block, down_matrix, preferred_element_type=jnp.float32)  10.1 us
    unnamed x19, local copies, waits for them, and re-layouts  7.48 us
    dot_general x1, matrix products, local(): up_part = jnp.dot(row_block, up_matrix, preferred_element_type=jnp.float32)  6.58 us
  transfers between devices with their start and end apart: 2, of which 2 were waited for; matrix products, arithmetic and copies ran while one was open for 0% of the time, Pallas kernels for 0%

profile of v1, /device:TPU:0, one launch (start us, length us, event | category | flops | bytes accessed | tf_op | source)
XLA Modules:
  0.0 215.0 jit_solution(9776257357133030426)
XLA Ops:
  6.5 0.0 copy-start
  6.5 0.0 all-gather.2.cloned.1.call-start
  6.6 0.8 reduce_max.9
  7.4 0.7 fusion.17
  8.1 0.7 fusion.16
  8.8 0.8 copy.26
  9.6 0.1 eq.44
  9.7 0.1 fusion.10
  9.8 0.1 reduce_window_sum.11
  9.9 0.2 select_reduce_fusion.1
  10.0 0.1 reduce_sum.39
  10.2 0.1 copy.27
  10.2 0.7 multiply_add_fusion
  10.9 0.1 convert_reduce_fusion
  11.0 0.1 broadcast_multiply_fusion.1
  11.2 0.6 sine_multiply_fusion
  11.7 0.0 copy-start.1
  11.7 1.2 copy-done.1
  13.0 0.0 copy-start.2
  13.0 0.9 copy-done.2
  13.9 0.0 copy-start.3
  13.9 0.9 copy-done.3
  14.8 0.0 copy-start.4
  14.8 0.8 copy-done.4
  15.6 0.0 copy-start.5
  15.6 0.8 copy-done.5
  16.4 0.0 copy-start.6
  16.4 0.7 copy-done.6
  17.1 0.0 copy-start.7
  17.1 0.7 copy-done.7
  17.8 0.7 copy-done.8
  18.5 51.4 %attention.1 = (f32[32,2048]{1,0:T(8,128)S(1)}, bf16[32,2048]{1,0:T(8,128)(2,1)S(1)}) custom-call(bf16[256,256]{1,0:T(8,128)(2,1)S(1)} %copy-done.2, bf16[256,128]{1,0:T(8,128)(2,1)S(1)} %copy-done.4, bf16[256,128]{1,0:T(8,128)(2,1)S(1)} %copy-done.5, f32[1,128]{1,0:T(1,128)S(1)} %bitcast.23, f32[1,128]{1,0:T(1,128)S(1)} %bitcast.24, ...), custom_call_target="tpu_custom_call" | custom-call | tf_op jit(solution)/shard_map/attention/pallas_call | solution.py:234
  69.9 0.3 convolution_convert_fusion.1
  70.2 0.2 reshape.126
  70.4 22.7 %all_to_all.10 = bf16[32,4,2048]{2,1,0:T(4,128)(2,1)S(1)} all-to-all(bf16[32,4,2048]{2,1,0:T(4,128)(2,1)S(1)} %reshape.126), channel_id=1, replica_groups=mesh['sp'=32,'tp'=8] {'sp'}, dimensions={0} | all-to-all | bytes 1048576 | tf_op jit(solution)/shard_map/all_to_all | solution.py:316
  93.1 0.9 reshape.127
  94.0 0.0 all-gather.2.cloned.1.call-update
  94.1 0.2 reduce-scatter.2.cloned.1.call-start
  94.3 29.5 %all-gather.2.cloned.1.call-done = bf16[1024,2048]{1,0:T(8,128)(2,1)} async-done(((bf16[128,2048]{1,0:T(8,128)(2,1)}), bf16[1024,2048]{1,0:T(8,128)(2,1)}) %all-gather.2.cloned.1.call-update) | async-done | bytes 4194320 | tf_op jit(solution)/shard_map/all_gather | solution.py:317
  123.8 6.6 %fusion.2 = f32[1024,512]{1,0:T(8,128)} fusion(bf16[1024,2048]{1,0:T(8,128)(2,1)} %all-gather.2.cloned.1.call-done, bf16[1,2048,512]{2,1,0:T(8,128)(2,1)} %param.24), kind=kOutput, calls=%fused_computation.5 | convolution fusion | flops 2147483648 | bytes 8388608 | tf_op jit(solution)/shard_map/dot_general | solution.py:319
  130.4 0.0 copy-done
  130.4 10.1 %convolution_convert_fusion = bf16[1024,2048]{1,0:T(8,128)(2,1)} fusion(bf16[1,512,2048]{2,1,0:T(8,128)(2,1)S(1)} %copy-done, f32[1024,512]{1,0:T(8,128)} %fusion.2, bf16[1024,2048]{1,0:T(8,128)(2,1)} %all-gather.2.cloned.1.call-done, bf16[1,2048,512]{2,1,0:T(8,128)(2,1)} %param.23), kind=kOutput, calls=%fused_computation | convolution fusion | flops 4300210176 | bytes 14680064 | tf_op jit(solution)/shard_map/dot_general | solution.py:323
  140.5 0.0 reduce-scatter.2.cloned.1.call-update
  140.5 40.6 %reduce-scatter.2.cloned.1.call-done = bf16[128,2048]{1,0:T(8,128)(2,1)} async-done(((bf16[1024,2048]{1,0:T(8,128)(2,1)}), bf16[128,2048]{1,0:T(8,128)(2,1)}) %reduce-scatter.2.cloned.1.call-update) | async-done | bytes 524304 | tf_op jit(solution)/shard_map/reduce_scatter | solution.py:322
  181.1 1.2 reshape.128
  182.4 24.8 %all_to_all.11 = bf16[32,4,2048]{2,1,0:T(4,128)(2,1)S(1)} all-to-all(bf16[32,4,2048]{2,1,0:T(4,128)(2,1)S(1)} %reshape.128), channel_id=1, replica_groups=mesh['sp'=32,'tp'=8] {'sp'}, dimensions={0} | all-to-all | bytes 1048576 | tf_op jit(solution)/shard_map/all_to_all | solution.py:328
  207.1 0.1 reshape.129
  207.3 0.9 fusion
  (4 shorter events, 0.0 us)
Async XLA Ops:
  6.5 123.9 %copy-start = (bf16[1,512,2048]{2,1,0:T(8,128)(2,1)S(1)}, bf16[1,512,2048]{2,1,0:T(8,128)(2,1)}, u32[]{:S(2)}) copy-start(bf16[1,512,2048]{2,1,0:T(8,128)(2,1)} %param.25) | copy-start | bytes 6291460
  6.5 117.3 %all-gather.2.cloned.1.call-start = ((), (), s32[]{:S(2)}) async-start(), calls=%async_computation.3 | async-start | bytes 4718592 | tf_op jit(solution)/shard_map/all_gather | solution.py:317
  11.7 1.2 copy-start.1
  13.0 0.9 copy-start.2
  13.9 0.9 copy-start.3
  14.8 0.8 copy-start.4
  15.6 0.8 copy-start.5
  16.4 0.7 copy-start.6
  17.1 0.7 copy-start.7
  17.8 0.7 copy-start.8
  94.1 87.1 %reduce-scatter.2.cloned.1.call-start = ((), (), s32[]{:S(2)}) async-start(), calls=%async_computation.4 | async-start | bytes 4718592 | tf_op jit(solution)/shard_map/reduce_scatter | solution.py:322
Sparse Core Ops, SparseCore 0:
  94.2 29.5 all-gather.1
  140.6 40.4 reduce-scatter.1

commit v2 on v1

--- a/solution.py
+++ b/solution.py
@@ -1,6 +1,7 @@
 import functools
 import jax
 import jax.numpy as jnp
+import numpy as np
 from jax import lax
 from jax.experimental import pallas as pl
 from jax.experimental.pallas import tpu as pltpu
@@ -29,14 +30,17 @@
     )
 
 
-def turn_tables(token_positions):
+EXPERTS, CAP = 32, 4
+BACK = (0, 1, -1, 2, -2, 3, -3, 4)
+
+
+def turn_tables():
     freq_count = HEAD_WIDTH // 4
-    frequency = ROPE_BASE ** (-jnp.arange(freq_count, dtype=jnp.float32) / freq_count)
-    row = (token_positions // GRID_W).astype(jnp.float32)[:, None] * frequency
-    col = (token_positions % GRID_W).astype(jnp.float32)[:, None] * frequency
-    angles = jnp.concatenate([row, row, col, col], axis=-1)
-    sign = jnp.where((jnp.arange(HEAD_WIDTH) // freq_count) % 2 == 0, -1.0, 1.0)
-    return jnp.cos(angles), jnp.sin(angles) * sign.astype(jnp.float32)
+    frequency = np.power(ROPE_BASE, -np.arange(freq_count) / freq_count).astype(np.float32)
+    place = np.arange(N_SP * SEQ // GRID_W, dtype=np.float32)
+    angles = np.tile(place[:, None] * frequency, (1, 4)).astype(np.float64)
+    sign = np.where((np.arange(HEAD_WIDTH) // freq_count) % 2 == 0, -1.0, 1.0)
+    return jnp.asarray(np.stack([np.cos(angles), np.sin(angles) * sign]).astype(np.float32))
 
 
 def turned(values, gain, cos, sin):
@@ -48,11 +52,20 @@
     return (normed * cos + partner * sin).astype(jnp.bfloat16)
 
 
-def attention_kernel(
-    q_ref, k_ref, v_ref, qg_ref, kg_ref, cos_ref, sin_ref, w_ref, x_ref, fg_ref,
-    mid_ref, normed_ref,
+def iota(shape, dim):
+    return lax.broadcasted_iota(jnp.int32, shape, dim)
+
+
+def layer_kernel(
+    q_hbm, k_hbm, v_hbm, gains_hbm, table_hbm, w_hbm, x_hbm, fg_hbm, routing_hbm, scores_hbm,
+    gate_hbm, up_hbm, down_hbm,
+    out_ref,
+    q_ref, k_ref, gains_ref, table_ref, x_ref, fg_ref, routing_ref, scores_ref,
+    wg, wu, wd,
     kv, qs, m_ref, l_ref, acc, wfull, att, att_in,
-    send_sem, recv_a, recv_b, recv_w, recv_att, own_sem,
+    slots, rows_in, xr, parts, parts_in, near_out, far_in, near_in, back, returned, middle_ref,
+    send_sem, recv_a, recv_b, recv_w, recv_att, load_sem,
+    recv_x, recv_part, recv_far, recv_near, recv_back,
 ):
     sp = lax.axis_index("sp")
     tp = lax.axis_index("tp")
@@ -65,26 +78,56 @@
     def tp_of(dy, other=False):
         return ((y + dy + NY) % NY) * 2 + ((1 - c) if other else c)
 
-    own_w = pltpu.make_async_copy(w_ref, wfull.at[tp], own_sem)
-    own_w.start()
+    loads = {}
+    for n, (name, src, dst) in enumerate((
+        ("k", k_hbm, k_ref), ("v", v_hbm, kv.at[sp, :, pl.ds(128, 128)]), ("gains", gains_hbm, gains_ref),
+        ("table", table_hbm, table_ref), ("q", q_hbm, q_ref),
+        ("w", w_hbm, wfull.at[tp]), ("x", x_hbm, x_ref), ("fg", fg_hbm, fg_ref),
+        ("routing", routing_hbm, routing_ref), ("scores", scores_hbm, scores_ref),
+        ("gate", gate_hbm.at[0], wg), ("up", up_hbm.at[0], wu), ("down", down_hbm.at[0], wd),
+    )):
+        loads[name] = pltpu.make_async_copy(src, dst, load_sem.at[n])
+        loads[name].start()
 
     barrier = pltpu.get_barrier_semaphore()
-    friends = [(sp_of(dz, dx), tp) for dz, dx in ((1, 0), (-1, 0), (0, 1), (0, -1), (0, 2))]
-    friends += [(sp, tp_of(dy, o)) for dy in range(NY) for o in (False, True) if (dy, o) != (0, False)]
-    for dev in friends:
-        pl.semaphore_signal(barrier, inc=1, device_id=dev, device_id_type=MESH)
-
-    cos, sin = cos_ref[...], sin_ref[...]
-    kv[sp, :, 0:128] = turned(k_ref[...].astype(jnp.float32), kg_ref[...], cos, sin)
-    kv[sp, :, 128:256] = v_ref[...]
+
+    def greet(i, carry):
+        pl.semaphore_signal(barrier, inc=1, device_id=((sp + i) % N_SP, tp), device_id_type=MESH)
+        return carry
+
+    lax.fori_loop(1, N_SP, greet, 0)
+
+    def greet_tp(i, carry):
+        pl.semaphore_signal(barrier, inc=1, device_id=(sp, (tp + i) % N_TP), device_id_type=MESH)
+        return carry
+
+    lax.fori_loop(1, N_TP, greet_tp, 0)
+
+    for name in ("k", "v", "gains", "table"):
+        loads[name].wait()
+
+    def table(which):
+        lane = iota((GRID_W, 128), 1)
+        cols = table_ref[which, 0:GRID_W, :]
+        return jnp.concatenate(
+            [
+                jnp.where(lane < 64, table_ref[which, pl.ds(sp * (SEQ // GRID_W) + i, 1), :], cols)
+                for i in range(SEQ // GRID_W)
+            ],
+            axis=0,
+        )
+
+    cos, sin = table(0), table(1)
+    kv[sp, :, 0:128] = turned(k_ref[...].astype(jnp.float32), gains_ref[1:2, :], cos, sin)
+    loads["q"].wait()
     for h in range(2):
         qs[h] = turned(
-            q_ref[:, h * 128 : (h + 1) * 128].astype(jnp.float32), qg_ref[...], cos, sin
+            q_ref[:, h * 128 : (h + 1) * 128].astype(jnp.float32), gains_ref[0:1, :], cos, sin
         )
     m_ref[...] = jnp.full(m_ref.shape, NEG_LARGE, jnp.float32)
     l_ref[...] = jnp.zeros(l_ref.shape, jnp.float32)
     acc[...] = jnp.zeros(acc.shape, jnp.float32)
-    pl.semaphore_wait(barrier, len(friends))
+    pl.semaphore_wait(barrier, N_SP + N_TP - 2)
 
     sent = []
 
@@ -144,10 +187,10 @@
         pass_on(half, dz, dx, link)
     for half, dev in ((0, tp_of(1)), (1, tp_of(-1)), (1, tp_of(1)), (0, tp_of(-1))):
         dst, recv = w_half(tp, half)
-        send(w_ref.at[pl.ds(half * 128, 128)], dst, recv, (sp, dev))
+        send(w_hbm.at[pl.ds(half * 128, 128)], dst, recv, (sp, dev))
     for half in (0, 1):
         dst, recv = w_half(tp, half)
-        send(w_ref.at[pl.ds(half * 128, 128)], dst, recv, (sp, tp_of(0, True)))
+        send(w_hbm.at[pl.ds(half * 128, 128)], dst, recv, (sp, tp_of(0, True)))
 
     def w_event(dy, half, links):
         ref, recv = w_half(tp_of(dy), half)
@@ -184,7 +227,6 @@
 
     left = {dz: (6 if dz == 0 else 8) for dz in (0, 1, -1, 2, -2, 3, -3, 4)}
     w_plan = {24: ((-1, 0, (1, 0)), (1, 1, (-1, 0))), 55: ((-1, 1, (0,)), (1, 0, (0,)))}
-    ready = []
     for count, (half, dz, dx) in enumerate(ARRIVALS):
         ref, recv = piece(half, sp_of(dz, dx))
         arrived(ref, recv)
@@ -205,7 +247,40 @@
         to = tp_of(dy, other)
         send(att.at[pl.ds(to * 32, 32)], att_in.at[tp], recv_att.at[tp], (sp, to))
 
-    own_w.wait()
+    for name in ("routing", "scores"):
+        loads[name].wait()
+    expert_no = iota((32, EXPERTS), 1)
+    first = (routing_ref[:, 0:1] == expert_no).astype(jnp.float32)
+    second = (routing_ref[:, 1:2] == expert_no).astype(jnp.float32)
+    top = jnp.maximum(scores_ref[:, 0:1], scores_ref[:, 1:2])
+    e0, e1 = jnp.exp(scores_ref[:, 0:1] - top), jnp.exp(scores_ref[:, 1:2] - top)
+    gates = first * (e0 / (e0 + e1)) + second * (e1 / (e0 + e1))
+    named = first + second
+    before = (iota((32, 32), 1) < iota((32, 32), 0)).astype(jnp.bfloat16)
+    rank = jnp.dot(before, named.astype(jnp.bfloat16), preferred_element_type=jnp.float32)
+    slot = jnp.where(named > 0.5, rank, -1.0)
+    slot4 = jnp.concatenate([slot] * 4, axis=0).astype(jnp.bfloat16)
+    gates4 = jnp.concatenate([gates] * 4, axis=0)
+    spread = (iota((512, EXPERTS), 0) // 16 == iota((512, EXPERTS), 1)).astype(jnp.bfloat16)
+    contract = (((1,), (1,)), ((), ()))
+    slot_rows = lax.dot_general(spread, slot4, contract, preferred_element_type=jnp.float32)
+    row = iota((512, 128), 0)
+    pick = (
+        (slot_rows == (row % 4).astype(jnp.float32)) & ((row // 4) % 4 == iota((512, 128), 1) // 32)
+    ).astype(jnp.bfloat16)
+    slot_cols = lax.dot_general(slot4, spread, contract, preferred_element_type=jnp.float32)
+    gate_cols = lax.dot_general(
+        gates4, spread.astype(jnp.float32), contract, preferred_element_type=jnp.float32,
+        precision=lax.Precision.HIGHEST,
+    )
+    col = iota((128, 512), 1)
+    merge = jnp.where(
+        (slot_cols == (col % 4).astype(jnp.float32)) & ((col // 4) % 4 == iota((128, 512), 0) // 32),
+        gate_cols, 0.0,
+    )
+
+    for name in ("w", "x", "fg"):
+        loads[name].wait()
     w_event(2, 0, (0,))
     w_event(2, 1, (0,))
     total = jnp.zeros((32, 2048), jnp.float32)
@@ -221,48 +296,153 @@
         part = jnp.dot(att_in[owner], wfull[owner], preferred_element_type=jnp.float32)
         total = total + part.astype(jnp.bfloat16).astype(jnp.float32)
     middle = x_ref[...].astype(jnp.float32) + total.astype(jnp.bfloat16).astype(jnp.float32)
-    mid_ref[...] = middle
-    normed_ref[...] = rms_scale(middle, fg_ref[...]).astype(jnp.bfloat16)
+    middle_ref[...] = middle
+    normed = rms_scale(middle, fg_ref[...]).astype(jnp.bfloat16)
+
+    stacked = jnp.concatenate([normed[:, 512 * j : 512 * (j + 1)] for j in range(4)], axis=0)
+    slots[...] = (
+        jnp.dot(pick, stacked, preferred_element_type=jnp.float32)
+        .astype(jnp.bfloat16)
+        .reshape(EXPERTS, 16, 512)
+    )
+    rows_in[tp, 0, x] = slots[sp]
+    for g, dz in enumerate(BACK):
+        for dx in (0, 1, -1, 2):
+            if (dz, dx) != (0, 0):
+                to = sp_of(-dz, -dx)
+                send(slots.at[to], rows_in.at[tp, g, x], recv_x.at[tp, g], (to, tp))
+
+    out_no, in_no = iota((128, 128), 0), iota((128, 128), 1)
+    sort = (
+        in_no == (out_no % 32 // 4) * 16 + (out_no // 32) * 4 + out_no % 4
+    ).astype(jnp.bfloat16)
+    out_no, in_no = in_no, out_no
+    unsort = (
+        in_no == (out_no % 32 // 4) * 16 + (out_no // 32) * 4 + out_no % 4
+    ).astype(jnp.bfloat16)
+
+    def group_of(owner, g):
+        return rows_in.at[owner, g], recv_x.at[owner, g]
+
+    def spread_rows(owner, g, links):
+        ref, recv = group_of(owner, g)
+        for link in links:
+            dev = tp_of(0, True) if link == 0 else tp_of(link)
+            send(ref, ref, recv, (sp, dev))
+
+    def own(g):
+        ref, recv = group_of(tp, g)
+        arrived(rows_in.at[tp, g, pl.ds(0, 3)] if g == 0 else ref, recv)
+        spread_rows(tp, g, (1, -1, 0))
+
+    def near(g):
+        for dy in (-1, 1):
+            owner = tp_of(dy)
+            arrived(*group_of(owner, g))
+            spread_rows(owner, g, ((-dy, 0) if (g % 2 == 0) == (dy == -1) else (0,)))
+
+    def far(g):
+        owner = tp_of(2)
+        arrived(*group_of(owner, g))
+        spread_rows(owner, g, (0,))
+
+    def other(g):
+        for dy in (0, -1, 1, 2):
+            arrived(*group_of(tp_of(dy, True), g))
+
+    def experts(o):
+        def sorted_rows(t, carry):
+            block = rows_in[t, pl.ds(2 * o, 2)].reshape(128, 512)
+            out = jnp.dot(sort, block, preferred_element_type=jnp.float32).astype(jnp.bfloat16)
+            at = pl.ds(pl.multiple_of(t * 32, 32), 32)
+            for j in range(4):
+                xr[at, 512 * j : 512 * (j + 1)] = out[32 * j : 32 * (j + 1)]
+            return carry
+
+        lax.fori_loop(0, N_TP, sorted_rows, 0)
+        rows = xr[...]
+        gate_part = jnp.dot(rows, wg[...], preferred_element_type=jnp.float32)
+        up_part = jnp.dot(rows, wu[...], preferred_element_type=jnp.float32)
+        hidden = (gate_part / (1.0 + jnp.exp(-gate_part)) * up_part).astype(jnp.bfloat16)
+        for j in range(4):
+            cols = slice(512 * j, 512 * (j + 1))
+            part = jnp.dot(hidden, wd[:, cols], preferred_element_type=jnp.float32)
+            parts[o, :, :, cols] = part.astype(jnp.bfloat16).reshape(N_TP, 32, 512)
+        for dy in (2, 1, -1, 0):
+            home = (y + dy + NY) % NY
+            send(
+                parts.at[o, tp_of(dy, True)], parts_in.at[o, home], recv_part.at[o, home],
+                (sp, tp_of(0, True)),
+            )
+
+    def chip_sum(o, dy):
+        home = (y + dy + NY) % NY
+        arrived(parts_in.at[o, home], recv_part.at[o, home])
+        return parts[o, tp_of(dy)].astype(jnp.float32) + parts_in[o, home].astype(jnp.float32)
+
+    def reduce_far(o):
+        near_out[o, 0] = chip_sum(o, 2).astype(jnp.bfloat16)
+        send(near_out.at[o, 0, pl.ds(0, 16)], far_in.at[o, 0], recv_far.at[o, 0], (sp, tp_of(1)))
+        send(near_out.at[o, 0, pl.ds(16, 16)], far_in.at[o, 1], recv_far.at[o, 1], (sp, tp_of(-1)))
+
+    def reduce_near(o):
+        for n, dy in ((0, 1), (1, -1)):
+            mine = chip_sum(o, dy)
+            arrived(far_in.at[o, n], recv_far.at[o, n])
+            at = slice(16 * n, 16 * n + 16)
+            rest = slice(16 - 16 * n, 32 - 16 * n)
+            near_out[o, 1 + n, at, :] = (
+                mine[at] + far_in[o, n].astype(jnp.float32)
+            ).astype(jnp.bfloat16)
+            near_out[o, 1 + n, rest, :] = mine[rest].astype(jnp.bfloat16)
+        for n, dy in ((0, 1), (1, -1)):
+            send(near_out.at[o, 1 + n], near_in.at[o, n], recv_near.at[o, n], (sp, tp_of(dy)))
+
+    def give_back(o):
+        whole = chip_sum(o, 0)
+        for n in (0, 1):
+            arrived(near_in.at[o, n], recv_near.at[o, n])
+            whole = whole + near_in[o, n].astype(jnp.float32)
+        result = whole.astype(jnp.bfloat16)
+        stack = jnp.concatenate([result[:, 512 * j : 512 * (j + 1)] for j in range(4)], axis=0)
+        back[o] = (
+            jnp.dot(unsort, stack, preferred_element_type=jnp.float32)
+            .astype(jnp.bfloat16)
+            .reshape(8, 16, 512)
+        )
+        if o == 0:
+            returned[sp] = back[0, x]
+        for n in (0, 1):
+            dz = BACK[2 * o + n]
+            for dx in (0, 1, -1, 2):
+                if (dz, dx) != (0, 0):
+                    to = sp_of(dz, dx)
+                    send(back.at[o, 4 * n + to % NX], returned.at[sp], recv_back, (to, tp))
+
+    own(0); own(1); own(2); near(0); own(3); near(1); far(0); own(4); near(2); far(1)
+    other(0); other(1)
+    for name in ("gate", "up", "down"):
+        loads[name].wait()
+    experts(0)
+    own(5); near(3); far(2); reduce_far(0); own(6); near(4); far(3); other(2); other(3)
+    experts(1)
+    reduce_near(0); own(7); near(5); far(4); reduce_far(1); near(6); far(5); other(4); other(5)
+    experts(2)
+    give_back(0); reduce_near(1); near(7); far(6); reduce_far(2); far(7); other(6); other(7)
+    experts(3)
+    give_back(1); reduce_near(2); reduce_far(3); give_back(2); reduce_near(3); give_back(3)
+
+    arrived(returned.at[pl.ds(0, N_SP - 1)], recv_back)
+    results = returned[...].reshape(512, 512)
+    routed = jnp.dot(
+        merge, results.astype(jnp.float32), preferred_element_type=jnp.float32,
+        precision=lax.Precision.HIGHEST,
+    )
+    for j in range(4):
+        cols = slice(512 * j, 512 * (j + 1))
+        out_ref[:, cols] = (middle_ref[:, cols] + routed[32 * j : 32 * (j + 1)]).astype(jnp.bfloat16)
     for copy in sent:
         copy.wait_send()
-
-
-def attention_part(x_resid, query_proj, keys, values, query_gain, key_gain, out_weight, ffn_gain):
-    positions = lax.axis_index("sp") * SEQ + jnp.arange(SEQ, dtype=jnp.int32)
-    cos, sin = turn_tables(positions)
-    vmem = pl.BlockSpec(memory_space=pltpu.VMEM)
-    return pl.pallas_call(
-        attention_kernel,
-        out_shape=(
-            jax.ShapeDtypeStruct((32, 2048), jnp.float32),
-            jax.ShapeDtypeStruct((32, 2048), jnp.bfloat16),
-        ),
-        in_specs=[vmem] * 7 + [pl.BlockSpec(memory_space=pl.ANY)] + [vmem] * 2,
-        out_specs=(vmem, vmem),
-        scratch_shapes=[
-            pltpu.VMEM((N_SP, SEQ, 256), jnp.bfloat16),
-            pltpu.VMEM((2, SEQ, 128), jnp.bfloat16),
-            pltpu.VMEM((2, SEQ, 128), jnp.float32),
-            pltpu.VMEM((2, SEQ, 128), jnp.float32),
-            pltpu.VMEM((2, SEQ, 128), jnp.float32),
-            pltpu.VMEM((N_TP, 256, 2048), jnp.bfloat16),
-            pltpu.VMEM((SEQ, 256), jnp.bfloat16),
-            pltpu.VMEM((N_TP, 32, 256), jnp.bfloat16),
-            pltpu.SemaphoreType.DMA((96,)),
-            pltpu.SemaphoreType.DMA((N_SP,)),
-            pltpu.SemaphoreType.DMA((N_SP,)),
-            pltpu.SemaphoreType.DMA((N_TP, 2)),
-            pltpu.SemaphoreType.DMA((N_TP,)),
-            pltpu.SemaphoreType.DMA,
-        ],
-        compiler_params=pltpu.CompilerParams(
-            collective_id=0, has_side_effects=True, vmem_limit_bytes=40 * 1024 * 1024
-        ),
-        name="attention",
-    )(
-        query_proj, keys, values, query_gain.reshape(1, -1), key_gain.reshape(1, -1), cos, sin,
-        out_weight, x_resid, ffn_gain.reshape(1, -1),
-    )
 
 
 def local(
@@ -280,62 +460,66 @@
     expert_up,
     expert_down,
 ):
-    own_tokens = x_resid.shape[0]
-    model_width = x_resid.shape[1]
-    middle, normed = attention_part(
-        x_resid, query_proj, projected_key_heads, projected_value_heads, query_gain,
-        key_norm_gain, out_weight, ffn_gain,
-    )
-    experts_all = lax.axis_size("sp") * expert_gate.shape[0]
-    capacity = max(2, 2 * own_tokens * TOP // experts_all)
-    flat_expert = routing.reshape(-1)
-    one_hot = (flat_expert[:, None] == jnp.arange(experts_all, dtype=jnp.int32)[None, :]).astype(
-        jnp.int32
-    )
-    earlier = jnp.cumsum(one_hot, axis=0) - one_hot
-    slot_rank = jnp.sum(earlier * one_hot, axis=1)
-    target = flat_expert * capacity + slot_rank
-    chooser = (
-        jnp.arange(experts_all * capacity, dtype=jnp.int32)[:, None] == target[None, :]
-    ).astype(jnp.float32)
-    gate_share = jax.nn.softmax(route_scores, axis=-1).reshape(-1)
-    picker = jnp.sum(chooser.reshape(experts_all * capacity, own_tokens, TOP), axis=2).astype(
-        jnp.bfloat16
-    )
-    combiner = jnp.sum(
-        (chooser * gate_share[None, :]).reshape(experts_all * capacity, own_tokens, TOP), axis=2
-    )
-    dispatch = (
-        jnp.dot(picker, normed, preferred_element_type=jnp.float32)
-        .astype(jnp.bfloat16)
-        .reshape(experts_all, capacity, model_width)
-    )
-    gate_matrix = expert_gate[0]
-    up_matrix = expert_up[0]
-    down_matrix = expert_down[0]
-    arrived = lax.all_to_all(dispatch, "sp", split_axis=0, concat_axis=0, tiled=True)
-    row_block = lax.all_gather(arrived.reshape(-1, model_width), "tp", axis=0, tiled=True)
-    gate_part = jnp.dot(row_block, gate_matrix, preferred_element_type=jnp.float32)
-    up_part = jnp.dot(row_block, up_matrix, preferred_element_type=jnp.float32)
-    hidden = (jax.nn.silu(gate_part) * up_part).astype(jnp.bfloat16)
-    row_block = hidden
-    expert_result = lax.psum_scatter(
-        jnp.dot(row_block, down_matrix, preferred_element_type=jnp.float32).astype(jnp.bfloat16),
-        "tp",
-        scatter_dimension=0,
-        tiled=True,
-    )
-    returned = lax.all_to_all(
-        expert_result.reshape(-1, capacity, model_width),
-        "sp",
-        split_axis=0,
-        concat_axis=0,
-        tiled=True,
-    )
-    routed = jnp.einsum(
-        "st,sd->td", combiner, returned.reshape(-1, model_width).astype(jnp.float32)
-    )
-    return (middle + routed).astype(jnp.bfloat16)
+    hbm = pl.BlockSpec(memory_space=pltpu.HBM)
+    bf16, f32 = jnp.bfloat16, jnp.float32
+    dma = pltpu.SemaphoreType.DMA
+    return pl.pallas_call(
+        layer_kernel,
+        out_shape=jax.ShapeDtypeStruct((32, 2048), bf16),
+        in_specs=[hbm] * 13,
+        out_specs=pl.BlockSpec(memory_space=pltpu.VMEM),
+        scratch_shapes=[
+            pltpu.VMEM((SEQ, 256), bf16),
+            pltpu.VMEM((SEQ, 128), bf16),
+            pltpu.VMEM((2, 128), f32),
+            pltpu.VMEM((2, 128, 128), f32),
+            pltpu.VMEM((32, 2048), bf16),
+            pltpu.VMEM((1, 2048), f32),
+            pltpu.VMEM((32, 2), jnp.int32),
+            pltpu.VMEM((32, 2), f32),
+            pltpu.VMEM((2048, 512), bf16),
+            pltpu.VMEM((2048, 512), bf16),
+            pltpu.VMEM((512, 2048), bf16),
+            pltpu.VMEM((N_SP, SEQ, 256), bf16),
+            pltpu.VMEM((2, SEQ, 128), bf16),
+            pltpu.VMEM((2, SEQ, 128), f32),
+            pltpu.VMEM((2, SEQ, 128), f32),
+            pltpu.VMEM((2, SEQ, 128), f32),
+            pltpu.VMEM((N_TP, 256, 2048), bf16),
+            pltpu.VMEM((SEQ, 256), bf16),
+            pltpu.VMEM((N_TP, 32, 256), bf16),
+            pltpu.VMEM((EXPERTS, 16, 512), bf16),
+            pltpu.VMEM((N_TP, 8, NX, 16, 512), bf16),
+            pltpu.VMEM((256, 2048), bf16),
+            pltpu.VMEM((4, N_TP, 32, 2048), bf16),
+            pltpu.VMEM((4, NY, 32, 2048), bf16),
+            pltpu.VMEM((4, 3, 32, 2048), bf16),
+            pltpu.VMEM((4, 2, 16, 2048), bf16),
+            pltpu.VMEM((4, 2, 32, 2048), bf16),
+            pltpu.VMEM((4, 8, 16, 512), bf16),
+            pltpu.VMEM((EXPERTS, 16, 512), bf16),
+            pltpu.VMEM((32, 2048), f32),
+            dma((256,)),
+            dma((N_SP,)),
+            dma((N_SP,)),
+            dma((N_TP, 2)),
+            dma((N_TP,)),
+            dma((13,)),
+            dma((N_TP, 8)),
+            dma((4, NY)),
+            dma((4, 2)),
+            dma((4, 2)),
+            dma,
+        ],
+        compiler_params=pltpu.CompilerParams(
+            collective_id=0, has_side_effects=True, vmem_limit_bytes=60 * 1024 * 1024
+        ),
+        name="layer",
+    )(
+        query_proj, projected_key_heads, projected_value_heads,
+        jnp.stack([query_gain, key_norm_gain]), turn_tables(), out_weight, x_resid,
+        ffn_gain.reshape(1, -1), routing, route_scores, expert_gate, expert_up, expert_down,
+    )
 
 
 def solution(mesh):

time: 217 us -> 139 us (0.64)
  Pallas kernels: 51.4 us -> 131 us
  waiting for transfers between devices: 70.2 us -> 0 us
  blocking collectives: 47.5 us -> 0 us
  matrix products: 17.9 us -> 0 us
  between operations: 13.5 us -> 0.01 us
  local copies, waits for them, and re-layouts: 10.2 us -> 4.29 us
  other arithmetic: 4.08 us -> 1.26 us
    pallas_call x1, Pallas kernels: 51.4 us -> 131 us  [local(): pl.pallas_call(layer_kernel, out_shape=jax.ShapeDtypeStruct((32, 2048), b...]
    all_to_all x2 -> x0, blocking collectives: 47.5 us -> none  [the longest x1 24.8 us: local(): lax.all_to_all(expert_result.reshape(-1, capacity, model_width), 'sp', sp...]
    reduce_scatter x1 -> x0, waiting for transfers between devices: 40.6 us -> none  [local(): lax.psum_scatter(jnp.dot(row_block, down_matrix, preferred_element_type=j...]
    all_gather x1 -> x0, waiting for transfers between devices: 29.5 us -> none  [local(): lax.all_gather(arrived.reshape(-1, model_width), 'tp', axis=0, tiled=True)]
    dot_general x4 -> x0, matrix products: 17.9 us -> none  [the longest x1 10.1 us: local(): jnp.dot(row_block, down_matrix, preferred_element_type=jnp.float32)]
    unnamed x19 -> x3, local copies, waits for them, and re-layouts: 7.48 us -> 4.29 us
    reshape x4 -> x0, local copies, waits for them, and re-layouts: 2.46 us -> none  [the longest x1 1.24 us: local(): expert_result.reshape(-1, capacity, model_width)]
  transfers between devices with their start and end apart: 2 -> 0, of which waited for: 2 -> 0; matrix products, arithmetic and copies ran while one was open for 0% -> 0% of each run, Pallas kernels for 0% -> 0%
where the time goes in v2:
time: 139 us; the launch traced here: 136 us
  Pallas kernels  131 us (94%)
  local copies, waits for them, and re-layouts  4.29 us (3%)
    pallas_call x1, Pallas kernels, local(): pl.pallas_call(layer_kernel, out_shape=jax.ShapeDtypeStruct((32, 2048), b...  131 us
    unnamed x3, local copies, waits for them, and re-layouts  4.29 us

profile of v2, /device:TPU:0, one launch (start us, length us, event | category | flops | bytes accessed | tf_op | source)
XLA Modules:
  0.0 136.1 jit_solution(3415341878365250641)
XLA Ops:
  0.0 1.3 pad_maximum_fusion.gains_hbm
  1.3 1.4 %copy.15.routing_hbm = s32[32,2]{1,0:T(8,128)} copy(s32[32,2]{0,1:T(2,128)} %param.22) | data formatting | bytes 512 | tf_op args[8]
  2.6 1.4 copy.16.scores_hbm
  4.0 130.5 %layer.1 = bf16[32,2048]{1,0:T(8,128)(2,1)} custom-call(bf16[256,256]{1,0:T(8,128)(2,1)} %q_hbm.1, bf16[256,128]{1,0:T(8,128)(2,1)} %k_hbm.1, bf16[256,128]{1,0:T(8,128)(2,1)} %v_hbm.1, f32[2,128]{1,0:T(2,128)} %pad_maximum_fusion.gains_hbm, f32[2,128,128]{2,1,0:T(8,128)} %constant.2.clone.table_hbm, bf16[256,2048]{1,0:T(8,128)(2,1)} %w_hbm.1, ...), custom_call_target="tpu_custom_call" | custom-call | tf_op jit(solution)/shard_map/layer/pallas_call | solution.py:466
  134.5 1.6 %copy.18 = bf16[32,2048]{1,0:T(8,128)(2,1)} copy(bf16[32,2048]{1,0:T(8,128)(2,1)} %layer.1) | data formatting | bytes 262144

commit v3 on v2

--- a/solution.py
+++ b/solution.py
@@ -21,7 +21,29 @@
 N_TP = NY * 2
 SEQ = 256
 ROWS_A = 96
-ARRIVALS = [('A', 0, 1), ('A', 0, -1), ('B', 1, 0), ('B', -1, 0), ('B', 0, -1), ('A', 1, 0), ('A', -1, 0), ('A', 0, 2), ('A', 1, 1), ('A', -1, 1), ('B', 0, 1), ('A', 1, -1), ('A', -1, -1), ('B', 1, -1), ('B', 1, 1), ('B', 2, 0), ('B', -2, 0), ('B', -1, -1), ('A', 2, 0), ('A', -2, 0), ('B', -1, 1), ('A', 1, 2), ('A', -1, 2), ('B', 1, 2), ('A', 2, 1), ('A', -2, 1), ('B', 0, 2), ('B', 2, -1), ('A', 2, -1), ('A', -2, -1), ('B', 2, 1), ('B', -2, -1), ('B', 3, 0), ('B', -3, 0), ('B', -2, 1), ('A', 3, 0), ('A', -3, 0), ('B', -1, 2), ('A', 2, 2), ('A', -2, 2), ('B', 2, 2), ('A', 3, 1), ('A', -3, 1), ('B', 3, -1), ('A', 3, -1), ('A', -3, -1), ('B', 3, 1), ('A', -3, 2), ('B', -3, -1), ('B', 4, 0), ('B', -3, 1), ('A', 4, 0), ('A', 4, -1), ('B', 3, 2), ('B', -2, 2), ('A', 3, 2), ('A', 4, 2), ('A', 4, 1), ('B', -3, 2), ('B', 4, 1), ('B', 4, -1), ('B', 4, 2)]
+ATTENTION_STEPS = (('A', 0, -1), ('A', 0, 1), ('B', -1, 0), ('B', 1, 0), ('A', 0, 2), ('A', -1, 0), ('A', 1, 0),
+    ('B', 0, -1), ('A', -1, -1), ('A', 1, -1), ('B', 0, 1), ('A', -1, 1), ('A', 1, 1), ('B', -1, -1),
+    ('B', -1, 1), ('B', -2, 0), ('B', 2, 0), ('B', 1, -1), ('A', -1, 2), ('A', 1, 2), ('B', 1, 1),
+    ('A', -2, 0), ('A', 2, 0), ('B', -1, 2), ('C', -1, 0), ('A', -2, -1), ('A', 2, -1), ('B', 0, 2),
+    ('C', -1, 1), ('A', -2, 1), ('A', 2, 1), ('B', -2, -1), ('C', 0, 0), ('B', -2, 1), ('C', 0, 1),
+    ('B', -3, 0), ('B', 3, 0), ('B', 2, -1), ('B', 2, 1), ('A', -2, 2), ('A', 2, 2), ('B', 1, 2),
+    ('C', 1, 0), ('A', 3, 0), ('A', -3, 0), ('C', 1, 1), ('A', -3, -1), ('A', 3, -1), ('B', -2, 2),
+    ('C', -2, 0), ('A', 3, 1), ('B', -3, -1), ('A', -3, 1), ('C', -2, 1), ('A', -3, 2), ('B', -3, 1),
+    ('B', 4, 0), ('B', 3, -1), ('B', 3, 1), ('A', 4, -1), ('A', 3, 2), ('A', 4, 0), ('B', -3, 2),
+    ('B', 2, 2), ('C', -3, 0), ('A', 4, 2), ('A', 4, 1), ('C', -3, 1), ('B', 4, 1), ('B', 4, -1),
+    ('C', 2, 0), ('C', 2, 1), ('B', 3, 2), ('C', 3, 0), ('C', 3, 1), ('B', 4, 2), ('C', 4, 0), ('C',
+    4, 1))
+EXPERT_STEPS = (('own', 0), ('own', 1), ('own', 2), ('near', 0, -1), ('near', 0, 1), ('near', 1, -1), ('near', 1,
+    1), ('own', 4), ('near', 2, -1), ('near', 2, 1), ('own', 3), ('far', 0), ('own', 6), ('far', 1),
+    ('near', 4, -1), ('near', 4, 1), ('sort', 0), ('own', 5), ('far', 2), ('up', 0, 0), ('near', 3,
+    1), ('up', 0, 1), ('near', 3, -1), ('down', 0, 0), ('near', 6, 1), ('down', 0, 1), ('near', 6,
+    -1), ('own', 7), ('near', 5, 1), ('far', 4), ('far', 3), ('near', 5, -1), ('rfar', 0), ('near', 7,
+    1), ('far', 6), ('sort', 1), ('up', 1, 0), ('near', 7, -1), ('far', 5), ('up', 1, 1), ('down', 1,
+    0), ('rnear', 0, 0), ('rnear', 0, 1), ('down', 1, 1), ('sort', 2), ('far', 7), ('up', 2, 0),
+    ('up', 2, 1), ('down', 2, 0), ('down', 2, 1), ('rfar', 1), ('sort', 3), ('up', 3, 0), ('back', 0),
+    ('up', 3, 1), ('down', 3, 0), ('rfar', 2), ('down', 3, 1), ('rnear', 1, 0), ('rnear', 1, 1),
+    ('rfar', 3), ('rnear', 2, 0), ('rnear', 2, 1), ('back', 1), ('rnear', 3, 0), ('rnear', 3, 1),
+    ('back', 2), ('back', 3))
 
 
 def rms_scale(values, norm_gain):
@@ -57,13 +79,13 @@
 
 
 def layer_kernel(
-    q_hbm, k_hbm, v_hbm, gains_hbm, table_hbm, w_hbm, x_hbm, fg_hbm, routing_hbm, scores_hbm,
+    q_hbm, k_hbm, v_hbm, qg_hbm, kg_hbm, table_hbm, w_hbm, x_hbm, fg_hbm, routing_hbm, scores_hbm,
     gate_hbm, up_hbm, down_hbm,
     out_ref,
-    q_ref, k_ref, gains_ref, table_ref, x_ref, fg_ref, routing_ref, scores_ref,
+    q_ref, k_ref, qg_ref, kg_ref, table_ref, x_ref, fg_ref, routing_ref, scores_ref,
     wg, wu, wd,
     kv, qs, m_ref, l_ref, acc, wfull, att, att_in,
-    slots, rows_in, xr, parts, parts_in, near_out, far_in, near_in, back, returned, middle_ref,
+    slots, rows_in, xr, hidden, parts, parts_in, near_out, far_in, near_in, back, returned, middle_ref,
     send_sem, recv_a, recv_b, recv_w, recv_att, load_sem,
     recv_x, recv_part, recv_far, recv_near, recv_back,
 ):
@@ -80,8 +102,8 @@
 
     loads = {}
     for n, (name, src, dst) in enumerate((
-        ("k", k_hbm, k_ref), ("v", v_hbm, kv.at[sp, :, pl.ds(128, 128)]), ("gains", gains_hbm, gains_ref),
-        ("table", table_hbm, table_ref), ("q", q_hbm, q_ref),
+        ("k", k_hbm, k_ref), ("v", v_hbm, kv.at[sp, :, pl.ds(128, 128)]), ("kg", kg_hbm, kg_ref),
+        ("table", table_hbm, table_ref), ("q", q_hbm, q_ref), ("qg", qg_hbm, qg_ref),
         ("w", w_hbm, wfull.at[tp]), ("x", x_hbm, x_ref), ("fg", fg_hbm, fg_ref),
         ("routing", routing_hbm, routing_ref), ("scores", scores_hbm, scores_ref),
         ("gate", gate_hbm.at[0], wg), ("up", up_hbm.at[0], wu), ("down", down_hbm.at[0], wd),
@@ -103,7 +125,7 @@
 
     lax.fori_loop(1, N_TP, greet_tp, 0)
 
-    for name in ("k", "v", "gains", "table"):
+    for name in ("k", "v", "kg", "table"):
         loads[name].wait()
 
     def table(which):
@@ -118,11 +140,12 @@
         )
 
     cos, sin = table(0), table(1)
-    kv[sp, :, 0:128] = turned(k_ref[...].astype(jnp.float32), gains_ref[1:2, :], cos, sin)
+    kv[sp, :, 0:128] = turned(k_ref[...].astype(jnp.float32), kg_ref[...], cos, sin)
     loads["q"].wait()
+    loads["qg"].wait()
     for h in range(2):
         qs[h] = turned(
-            q_ref[:, h * 128 : (h + 1) * 128].astype(jnp.float32), gains_ref[0:1, :], cos, sin
+            q_ref[:, h * 128 : (h + 1) * 128].astype(jnp.float32), qg_ref[...], cos, sin
         )
     m_ref[...] = jnp.full(m_ref.shape, NEG_LARGE, jnp.float32)
     l_ref[...] = jnp.zeros(l_ref.shape, jnp.float32)
@@ -201,42 +224,37 @@
 
     scale2 = HEAD_WIDTH ** (-0.5) * LOG2E
 
-    def attend(group):
-        def step(i, carry):
-            block = kv[pl.ds(group * NX + 2 * i, 2)].reshape(2 * SEQ, 256)
-            keys, values = block[:, 0:128], block[:, 128:256]
-            for h in range(2):
-                s = lax.dot_general(
-                    qs[h], keys, (((1,), (1,)), ((), ())), preferred_element_type=jnp.float32
-                )
-                m_old = m_ref[h]
-                m_new = jnp.maximum(m_old, jnp.max(s, axis=1, keepdims=True))
-                alpha = jnp.exp2((m_old - m_new) * scale2)
-                m_all = jnp.concatenate([m_new * scale2] * 4, axis=1)
-                p = jnp.exp2(s * scale2 - m_all)
-                l_ref[h] = l_ref[h] * alpha + (
-                    (p[:, 0:128] + p[:, 128:256]) + (p[:, 256:384] + p[:, 384:512])
-                )
-                acc[h] = acc[h] * alpha + jnp.dot(
-                    p.astype(jnp.bfloat16), values, preferred_element_type=jnp.float32
-                )
-                m_ref[h] = m_new
-            return carry
-
-        lax.fori_loop(0, NX // 2, step, 0)
-
-    left = {dz: (6 if dz == 0 else 8) for dz in (0, 1, -1, 2, -2, 3, -3, 4)}
-    w_plan = {24: ((-1, 0, (1, 0)), (1, 1, (-1, 0))), 55: ((-1, 1, (0,)), (1, 0, (0,)))}
-    for count, (half, dz, dx) in enumerate(ARRIVALS):
-        ref, recv = piece(half, sp_of(dz, dx))
-        arrived(ref, recv)
-        for link in next_links(half, dz, dx):
-            pass_on(half, dz, dx, link)
+    def attend(group, i):
+        block = kv[pl.ds(group * NX + 2 * i, 2)].reshape(2 * SEQ, 256)
+        keys, values = block[:, 0:128], block[:, 128:256]
+        for h in range(2):
+            s = lax.dot_general(
+                qs[h], keys, (((1,), (1,)), ((), ())), preferred_element_type=jnp.float32
+            )
+            m_old = m_ref[h]
+            m_new = jnp.maximum(m_old, jnp.max(s, axis=1, keepdims=True))
+            alpha = jnp.exp2((m_old - m_new) * scale2)
+            m_all = jnp.concatenate([m_new * scale2] * 4, axis=1)
+            p = jnp.exp2(s * scale2 - m_all)
+            l_ref[h] = l_ref[h] * alpha + (
+                (p[:, 0:128] + p[:, 128:256]) + (p[:, 256:384] + p[:, 384:512])
+            )
+            acc[h] = acc[h] * alpha + jnp.dot(
+                p.astype(jnp.bfloat16), values, preferred_element_type=jnp.float32
+            )
+            m_ref[h] = m_new
+
+    w_plan = {30: ((-1, 0, (1, 0)), (1, 1, (-1, 0))), 70: ((-1, 1, (0,)), (1, 0, (0,)))}
+    for count, (half, dz, dx) in enumerate(ATTENTION_STEPS):
+        if half == "C":
+            attend((z - dz + NZ) % NZ, dx)
+        else:
+            ref, recv = piece(half, sp_of(dz, dx))
+            arrived(ref, recv)
+            for link in next_links(half, dz, dx):
+                pass_on(half, dz, dx, link)
         for dy, w_part, links in w_plan.get(count, ()):
             w_event(dy, w_part, links)
-        left[dz] -= 1
-        if left[dz] == 0:
-            attend((z - dz + NZ) % NZ)
 
     for h in range(2):
         total = jnp.sum(l_ref[h], axis=1, keepdims=True)
@@ -249,42 +267,45 @@
 
     for name in ("routing", "scores"):
         loads[name].wait()
-    expert_no = iota((32, EXPERTS), 1)
-    first = (routing_ref[:, 0:1] == expert_no).astype(jnp.float32)
-    second = (routing_ref[:, 1:2] == expert_no).astype(jnp.float32)
-    top = jnp.maximum(scores_ref[:, 0:1], scores_ref[:, 1:2])
-    e0, e1 = jnp.exp(scores_ref[:, 0:1] - top), jnp.exp(scores_ref[:, 1:2] - top)
+    expert_no = iota((EXPERTS, 32), 0)
+    first = (routing_ref[0:1, :] == expert_no).astype(jnp.float32)
+    second = (routing_ref[1:2, :] == expert_no).astype(jnp.float32)
+    top = jnp.maximum(scores_ref[0:1, :], scores_ref[1:2, :])
+    e0, e1 = jnp.exp(scores_ref[0:1, :] - top), jnp.exp(scores_ref[1:2, :] - top)
     gates = first * (e0 / (e0 + e1)) + second * (e1 / (e0 + e1))
     named = first + second
-    before = (iota((32, 32), 1) < iota((32, 32), 0)).astype(jnp.bfloat16)
-    rank = jnp.dot(before, named.astype(jnp.bfloat16), preferred_element_type=jnp.float32)
-    slot = jnp.where(named > 0.5, rank, -1.0)
-    slot4 = jnp.concatenate([slot] * 4, axis=0).astype(jnp.bfloat16)
-    gates4 = jnp.concatenate([gates] * 4, axis=0)
+    before = (iota((32, 32), 0) < iota((32, 32), 1)).astype(jnp.bfloat16)
+    rank = jnp.dot(named.astype(jnp.bfloat16), before, preferred_element_type=jnp.float32)
+    slot = jnp.where(named > 0.5, rank, -1.0).astype(jnp.bfloat16)
+    again = (iota((32, 128), 1) % 32 == iota((32, 128), 0)).astype(jnp.bfloat16)
+    slot4 = jnp.dot(slot, again, preferred_element_type=jnp.float32).astype(jnp.bfloat16)
+    gates4 = jnp.dot(
+        gates, again.astype(jnp.float32), preferred_element_type=jnp.float32,
+        precision=lax.Precision.HIGHEST,
+    )
     spread = (iota((512, EXPERTS), 0) // 16 == iota((512, EXPERTS), 1)).astype(jnp.bfloat16)
-    contract = (((1,), (1,)), ((), ()))
-    slot_rows = lax.dot_general(spread, slot4, contract, preferred_element_type=jnp.float32)
+    slot_rows = jnp.dot(spread, slot4, preferred_element_type=jnp.float32)
     row = iota((512, 128), 0)
-    pick = (
-        (slot_rows == (row % 4).astype(jnp.float32)) & ((row // 4) % 4 == iota((512, 128), 1) // 32)
-    ).astype(jnp.bfloat16)
-    slot_cols = lax.dot_general(slot4, spread, contract, preferred_element_type=jnp.float32)
-    gate_cols = lax.dot_general(
-        gates4, spread.astype(jnp.float32), contract, preferred_element_type=jnp.float32,
-        precision=lax.Precision.HIGHEST,
-    )
-    col = iota((128, 512), 1)
-    merge = jnp.where(
-        (slot_cols == (col % 4).astype(jnp.float32)) & ((col // 4) % 4 == iota((128, 512), 0) // 32),
-        gate_cols, 0.0,
-    )
+    held = (slot_rows == (row % 4).astype(jnp.float32)) & (
+        (row // 4) % 4 == iota((512, 128), 1) // 32
+    )
+    pick = held.astype(jnp.bfloat16)
+    merge_rows = jnp.where(
+        held,
+        jnp.dot(
+            spread.astype(jnp.float32), gates4, preferred_element_type=jnp.float32,
+            precision=lax.Precision.HIGHEST,
+        ),
+        0.0,
+    )
+    merge = merge_rows.T
 
     for name in ("w", "x", "fg"):
         loads[name].wait()
     w_event(2, 0, (0,))
     w_event(2, 1, (0,))
     total = jnp.zeros((32, 2048), jnp.float32)
-    order = [(0, False), (0, True), (1, False), (3, False), (1, True), (3, True), (2, False), (2, True)]
+    order = [(0, False), (1, False), (3, False), (2, False), (0, True), (1, True), (3, True), (2, True)]
     for dy, other in order:
         owner = tp_of(dy, other)
         if (dy, other) != (0, False):
@@ -335,22 +356,21 @@
         arrived(rows_in.at[tp, g, pl.ds(0, 3)] if g == 0 else ref, recv)
         spread_rows(tp, g, (1, -1, 0))
 
-    def near(g):
-        for dy in (-1, 1):
-            owner = tp_of(dy)
-            arrived(*group_of(owner, g))
-            spread_rows(owner, g, ((-dy, 0) if (g % 2 == 0) == (dy == -1) else (0,)))
+    def near(g, dy):
+        owner = tp_of(dy)
+        arrived(*group_of(owner, g))
+        spread_rows(owner, g, ((-dy, 0) if (g % 2 == 0) == (dy == -1) else (0,)))
 
     def far(g):
         owner = tp_of(2)
         arrived(*group_of(owner, g))
         spread_rows(owner, g, (0,))
 
-    def other(g):
-        for dy in (0, -1, 1, 2):
-            arrived(*group_of(tp_of(dy, True), g))
-
-    def experts(o):
+    def sort_rows(o):
+        for g in (2 * o, 2 * o + 1):
+            for dy in (0, -1, 1, 2):
+                arrived(*group_of(tp_of(dy, True), g))
+
         def sorted_rows(t, carry):
             block = rows_in[t, pl.ds(2 * o, 2)].reshape(128, 512)
             out = jnp.dot(sort, block, preferred_element_type=jnp.float32).astype(jnp.bfloat16)
@@ -360,14 +380,23 @@
             return carry
 
         lax.fori_loop(0, N_TP, sorted_rows, 0)
-        rows = xr[...]
-        gate_part = jnp.dot(rows, wg[...], preferred_element_type=jnp.float32)
-        up_part = jnp.dot(rows, wu[...], preferred_element_type=jnp.float32)
-        hidden = (gate_part / (1.0 + jnp.exp(-gate_part)) * up_part).astype(jnp.bfloat16)
-        for j in range(4):
+
+    def up(o, n):
+        if (o, n) == (0, 0):
+            for name in ("gate", "up", "down"):
+                loads[name].wait()
+        cols = slice(256 * n, 256 * (n + 1))
+        gate_part = jnp.dot(xr[...], wg[:, cols], preferred_element_type=jnp.float32)
+        up_part = jnp.dot(xr[...], wu[:, cols], preferred_element_type=jnp.float32)
+        hidden[:, cols] = (gate_part / (1.0 + jnp.exp(-gate_part)) * up_part).astype(jnp.bfloat16)
+
+    def down(o, n):
+        for j in (2 * n, 2 * n + 1):
             cols = slice(512 * j, 512 * (j + 1))
-            part = jnp.dot(hidden, wd[:, cols], preferred_element_type=jnp.float32)
+            part = jnp.dot(hidden[...], wd[:, cols], preferred_element_type=jnp.float32)
             parts[o, :, :, cols] = part.astype(jnp.bfloat16).reshape(N_TP, 32, 512)
+        if (o, n) not in last_down:
+            return
         for dy in (2, 1, -1, 0):
             home = (y + dy + NY) % NY
             send(
@@ -375,9 +404,13 @@
                 (sp, tp_of(0, True)),
             )
 
+    from_partner = set()
+
     def chip_sum(o, dy):
         home = (y + dy + NY) % NY
-        arrived(parts_in.at[o, home], recv_part.at[o, home])
+        if (o, dy) not in from_partner:
+            arrived(parts_in.at[o, home], recv_part.at[o, home])
+            from_partner.add((o, dy))
         return parts[o, tp_of(dy)].astype(jnp.float32) + parts_in[o, home].astype(jnp.float32)
 
     def reduce_far(o):
@@ -385,18 +418,17 @@
         send(near_out.at[o, 0, pl.ds(0, 16)], far_in.at[o, 0], recv_far.at[o, 0], (sp, tp_of(1)))
         send(near_out.at[o, 0, pl.ds(16, 16)], far_in.at[o, 1], recv_far.at[o, 1], (sp, tp_of(-1)))
 
-    def reduce_near(o):
-        for n, dy in ((0, 1), (1, -1)):
-            mine = chip_sum(o, dy)
-            arrived(far_in.at[o, n], recv_far.at[o, n])
-            at = slice(16 * n, 16 * n + 16)
-            rest = slice(16 - 16 * n, 32 - 16 * n)
-            near_out[o, 1 + n, at, :] = (
-                mine[at] + far_in[o, n].astype(jnp.float32)
-            ).astype(jnp.bfloat16)
-            near_out[o, 1 + n, rest, :] = mine[rest].astype(jnp.bfloat16)
-        for n, dy in ((0, 1), (1, -1)):
-            send(near_out.at[o, 1 + n], near_in.at[o, n], recv_near.at[o, n], (sp, tp_of(dy)))
+    def reduce_near(o, n):
+        dy = (1, -1)[n]
+        mine = chip_sum(o, dy)
+        arrived(far_in.at[o, n], recv_far.at[o, n])
+        at = slice(16 * n, 16 * n + 16)
+        rest = slice(16 - 16 * n, 32 - 16 * n)
+        near_out[o, 1 + n, at, :] = (mine[at] + far_in[o, n].astype(jnp.float32)).astype(
+            jnp.bfloat16
+        )
+        near_out[o, 1 + n, rest, :] = mine[rest].astype(jnp.bfloat16)
+        send(near_out.at[o, 1 + n], near_in.at[o, n], recv_near.at[o, n], (sp, tp_of(dy)))
 
     def give_back(o):
         whole = chip_sum(o, 0)
@@ -419,18 +451,17 @@
                     to = sp_of(dz, dx)
                     send(back.at[o, 4 * n + to % NX], returned.at[sp], recv_back, (to, tp))
 
-    own(0); own(1); own(2); near(0); own(3); near(1); far(0); own(4); near(2); far(1)
-    other(0); other(1)
-    for name in ("gate", "up", "down"):
-        loads[name].wait()
-    experts(0)
-    own(5); near(3); far(2); reduce_far(0); own(6); near(4); far(3); other(2); other(3)
-    experts(1)
-    reduce_near(0); own(7); near(5); far(4); reduce_far(1); near(6); far(5); other(4); other(5)
-    experts(2)
-    give_back(0); reduce_near(1); near(7); far(6); reduce_far(2); far(7); other(6); other(7)
-    experts(3)
-    give_back(1); reduce_near(2); reduce_far(3); give_back(2); reduce_near(3); give_back(3)
+    last_down = {}
+    for kind, o, *n in EXPERT_STEPS:
+        if kind == "down":
+            last_down[o] = n[0]
+    last_down = set(last_down.items())
+    steps = dict(
+        own=own, near=near, far=far, sort=sort_rows, up=up, down=down, rfar=reduce_far,
+        rnear=reduce_near, back=give_back,
+    )
+    for kind, *args in EXPERT_STEPS:
+        steps[kind](*args)
 
     arrived(returned.at[pl.ds(0, N_SP - 1)], recv_back)
     results = returned[...].reshape(512, 512)
@@ -466,17 +497,18 @@
     return pl.pallas_call(
         layer_kernel,
         out_shape=jax.ShapeDtypeStruct((32, 2048), bf16),
-        in_specs=[hbm] * 13,
+        in_specs=[hbm] * 14,
         out_specs=pl.BlockSpec(memory_space=pltpu.VMEM),
         scratch_shapes=[
             pltpu.VMEM((SEQ, 256), bf16),
             pltpu.VMEM((SEQ, 128), bf16),
-            pltpu.VMEM((2, 128), f32),
+            pltpu.VMEM((1, 128), f32),
+            pltpu.VMEM((1, 128), f32),
             pltpu.VMEM((2, 128, 128), f32),
             pltpu.VMEM((32, 2048), bf16),
             pltpu.VMEM((1, 2048), f32),
-            pltpu.VMEM((32, 2), jnp.int32),
-            pltpu.VMEM((32, 2), f32),
+            pltpu.VMEM((2, 32), jnp.int32),
+            pltpu.VMEM((2, 32), f32),
             pltpu.VMEM((2048, 512), bf16),
             pltpu.VMEM((2048, 512), bf16),
             pltpu.VMEM((512, 2048), bf16),
@@ -491,6 +523,7 @@
             pltpu.VMEM((EXPERTS, 16, 512), bf16),
             pltpu.VMEM((N_TP, 8, NX, 16, 512), bf16),
             pltpu.VMEM((256, 2048), bf16),
+            pltpu.VMEM((256, 512), bf16),
             pltpu.VMEM((4, N_TP, 32, 2048), bf16),
             pltpu.VMEM((4, NY, 32, 2048), bf16),
             pltpu.VMEM((4, 3, 32, 2048), bf16),
@@ -504,7 +537,7 @@
             dma((N_SP,)),
             dma((N_TP, 2)),
             dma((N_TP,)),
-            dma((13,)),
+            dma((14,)),
             dma((N_TP, 8)),
             dma((4, NY)),
             dma((4, 2)),
@@ -517,8 +550,8 @@
         name="layer",
     )(
         query_proj, projected_key_heads, projected_value_heads,
-        jnp.stack([query_gain, key_norm_gain]), turn_tables(), out_weight, x_resid,
-        ffn_gain.reshape(1, -1), routing, route_scores, expert_gate, expert_up, expert_down,
+        query_gain.reshape(1, -1), key_norm_gain.reshape(1, -1), turn_tables(), out_weight, x_resid,
+        ffn_gain.reshape(1, -1), routing.T, route_scores.T, expert_gate, expert_up, expert_down,
     )
 
 

time: 139 us -> 117 us (0.84); the launches traced: 136 us -> 117 us
  Pallas kernels: 131 us -> 115 us
  local copies, waits for them, and re-layouts: 4.29 us -> 1.57 us
    pallas_call x1, Pallas kernels: 131 us -> 115 us  [local(): pl.pallas_call(layer_kernel, out_shape=jax.ShapeDtypeStruct((32, 2048), b...]
    unnamed x3 -> x1, local copies, waits for them, and re-layouts: 4.29 us -> 1.57 us
where the time goes in v3:
time: 117 us
  Pallas kernels  115 us (98%)
  local copies, waits for them, and re-layouts  1.57 us (1%)
    pallas_call x1, Pallas kernels, local(): pl.pallas_call(layer_kernel, out_shape=jax.ShapeDtypeStruct((32, 2048), b...  115 us

profile of v3, /device:TPU:0, one launch (start us, length us, event | category | flops | bytes accessed | tf_op | source)
XLA Modules:
  0.0 116.5 jit_solution(15302251106656270784)
XLA Ops:
  0.0 115.0 %layer.1 = bf16[32,2048]{1,0:T(8,128)(2,1)} custom-call(bf16[256,256]{1,0:T(8,128)(2,1)} %q_hbm.1, bf16[256,128]{1,0:T(8,128)(2,1)} %k_hbm.1, bf16[256,128]{1,0:T(8,128)(2,1)} %v_hbm.1, f32[1,128]{1,0:T(1,128)} %bitcast.8, f32[1,128]{1,0:T(1,128)} %bitcast.9, f32[2,128,128]{2,1,0:T(8,128)} %constant.2.clone.table_hbm, bf16[256,2048]{1,0:T(8,128)(2,1)} %w_hbm.1, ...), custom_call_target="tpu_custom_call" | custom-call | tf_op jit(solution)/shard_map/layer/pallas_call | solution.py:497
  115.0 1.6 %copy.16 = bf16[32,2048]{1,0:T(8,128)(2,1)} copy(bf16[32,2048]{1,0:T(8,128)(2,1)} %layer.1) | data formatting | bytes 262144

commit v4 on v3

--- a/solution.py
+++ b/solution.py
@@ -33,17 +33,17 @@
     ('B', 2, 2), ('C', -3, 0), ('A', 4, 2), ('A', 4, 1), ('C', -3, 1), ('B', 4, 1), ('B', 4, -1),
     ('C', 2, 0), ('C', 2, 1), ('B', 3, 2), ('C', 3, 0), ('C', 3, 1), ('B', 4, 2), ('C', 4, 0), ('C',
     4, 1))
-EXPERT_STEPS = (('own', 0), ('own', 1), ('own', 2), ('near', 0, -1), ('near', 0, 1), ('near', 1, -1), ('near', 1,
-    1), ('own', 4), ('near', 2, -1), ('near', 2, 1), ('own', 3), ('far', 0), ('own', 6), ('far', 1),
-    ('near', 4, -1), ('near', 4, 1), ('sort', 0), ('own', 5), ('far', 2), ('up', 0, 0), ('near', 3,
-    1), ('up', 0, 1), ('near', 3, -1), ('down', 0, 0), ('near', 6, 1), ('down', 0, 1), ('near', 6,
-    -1), ('own', 7), ('near', 5, 1), ('far', 4), ('far', 3), ('near', 5, -1), ('rfar', 0), ('near', 7,
-    1), ('far', 6), ('sort', 1), ('up', 1, 0), ('near', 7, -1), ('far', 5), ('up', 1, 1), ('down', 1,
-    0), ('rnear', 0, 0), ('rnear', 0, 1), ('down', 1, 1), ('sort', 2), ('far', 7), ('up', 2, 0),
-    ('up', 2, 1), ('down', 2, 0), ('down', 2, 1), ('rfar', 1), ('sort', 3), ('up', 3, 0), ('back', 0),
-    ('up', 3, 1), ('down', 3, 0), ('rfar', 2), ('down', 3, 1), ('rnear', 1, 0), ('rnear', 1, 1),
-    ('rfar', 3), ('rnear', 2, 0), ('rnear', 2, 1), ('back', 1), ('rnear', 3, 0), ('rnear', 3, 1),
-    ('back', 2), ('back', 3))
+EXPERT_STEPS = (('own', 0), ('own', 1), ('own', 3), ('near', 0, -1), ('near', 0, 1), ('near', 1, -1), ('near', 1,
+    1), ('own', 4), ('near', 3, -1), ('near', 3, 1), ('own', 2), ('far', 0), ('own', 5), ('far', 1),
+    ('near', 4, -1), ('near', 4, 1), ('near', 2, -1), ('own', 6), ('far', 3), ('near', 5, -1),
+    ('sort', 0), ('near', 2, 1), ('up', 0, 0), ('own', 7), ('far', 4), ('up', 0, 1), ('near', 5, 1),
+    ('down', 0, 0), ('far', 2), ('down', 0, 1), ('near', 6, 1), ('near', 6, -1), ('near', 7, 1),
+    ('near', 7, -1), ('far', 5), ('sort', 1), ('rfar', 0), ('up', 1, 0), ('far', 6), ('up', 1, 1),
+    ('far', 7), ('down', 1, 0), ('down', 1, 1), ('sort', 2), ('rnear', 0, 0), ('rnear', 0, 1), ('up',
+    2, 0), ('up', 2, 1), ('down', 2, 0), ('down', 2, 1), ('rfar', 1), ('sort', 3), ('up', 3, 0),
+    ('up', 3, 1), ('down', 3, 0), ('down', 3, 1), ('back', 0), ('rfar', 2), ('rnear', 1, 0), ('rnear',
+    1, 1), ('rfar', 3), ('rnear', 2, 0), ('rnear', 2, 1), ('back', 1), ('rnear', 3, 0), ('rnear', 3,
+    1), ('back', 2), ('back', 3))
 
 
 def rms_scale(values, norm_gain):
@@ -53,7 +53,9 @@
 
 
 EXPERTS, CAP = 32, 4
-BACK = (0, 1, -1, 2, -2, 3, -3, 4)
+BACK = (0, 1, 2, -1, -2, -3, 3, 4)
+AHEAD = (0, 1, -1, 2, -2, 3, -3, 4)
+KINDS = ("A", "B", "w", "att", "slots", "rows", "parts", "far", "near", "back")
 
 
 def turn_tables():
@@ -87,7 +89,7 @@
     kv, qs, m_ref, l_ref, acc, wfull, att, att_in,
     slots, rows_in, xr, hidden, parts, parts_in, near_out, far_in, near_in, back, returned, middle_ref,
     send_sem, recv_a, recv_b, recv_w, recv_att, load_sem,
-    recv_x, recv_part, recv_far, recv_near, recv_back,
+    recv_own, recv_y, recv_other, recv_part, recv_far, recv_near, recv_back,
 ):
     sp = lax.axis_index("sp")
     tp = lax.axis_index("tp")
@@ -113,11 +115,9 @@
 
     barrier = pltpu.get_barrier_semaphore()
 
-    def greet(i, carry):
-        pl.semaphore_signal(barrier, inc=1, device_id=((sp + i) % N_SP, tp), device_id_type=MESH)
-        return carry
-
-    lax.fori_loop(1, N_SP, greet, 0)
+    friends = [(sp_of(dz, dx), tp) for dz, dx in ((1, 0), (-1, 0), (0, 1), (0, -1), (0, 2))]
+    for dev in friends:
+        pl.semaphore_signal(barrier, inc=1, device_id=dev, device_id_type=MESH)
 
     def greet_tp(i, carry):
         pl.semaphore_signal(barrier, inc=1, device_id=(sp, (tp + i) % N_TP), device_id_type=MESH)
@@ -150,23 +150,25 @@
     m_ref[...] = jnp.full(m_ref.shape, NEG_LARGE, jnp.float32)
     l_ref[...] = jnp.zeros(l_ref.shape, jnp.float32)
     acc[...] = jnp.zeros(acc.shape, jnp.float32)
-    pl.semaphore_wait(barrier, N_SP + N_TP - 2)
-
-    sent = []
-
-    def send(src, dst, recv, dev):
-        copy = pltpu.make_async_remote_copy(
-            src_ref=src, dst_ref=dst, send_sem=send_sem.at[len(sent)], recv_sem=recv,
+    pl.semaphore_wait(barrier, len(friends) + N_TP - 1)
+
+    def send(kind, src, dst, recv, dev):
+        pltpu.make_async_remote_copy(
+            src_ref=src, dst_ref=dst, send_sem=send_sem.at[KINDS.index(kind)], recv_sem=recv,
             device_id=dev, device_id_type=MESH,
-        )
-        copy.start()
-        sent.append(copy)
+        ).start()
 
     def arrived(ref, recv):
         pltpu.make_async_remote_copy(
             src_ref=ref, dst_ref=ref, send_sem=send_sem.at[0], recv_sem=recv,
             device_id=(sp, tp_of(0, True)), device_id_type=MESH,
         ).wait_recv()
+
+    def all_sent(kind, ref):
+        pltpu.make_async_remote_copy(
+            src_ref=ref, dst_ref=ref, send_sem=send_sem.at[KINDS.index(kind)],
+            recv_sem=recv_back, device_id=(sp, tp_of(0, True)), device_id_type=MESH,
+        ).wait_send()
 
     def piece(half, owner):
         if half == "A":
@@ -179,7 +181,7 @@
             "z+": (sp_of(-1, 0), tp), "z-": (sp_of(1, 0), tp),
             "x+": (sp_of(0, -1), tp), "x-": (sp_of(0, 1), tp), "x2": (sp_of(0, 2), tp),
         }[link]
-        send(ref, ref, recv, dev)
+        send(half, ref, ref, recv, dev)
 
     def next_links(half, dz, dx):
         if half == "A":
@@ -210,17 +212,17 @@
         pass_on(half, dz, dx, link)
     for half, dev in ((0, tp_of(1)), (1, tp_of(-1)), (1, tp_of(1)), (0, tp_of(-1))):
         dst, recv = w_half(tp, half)
-        send(w_hbm.at[pl.ds(half * 128, 128)], dst, recv, (sp, dev))
+        send("w", w_hbm.at[pl.ds(half * 128, 128)], dst, recv, (sp, dev))
     for half in (0, 1):
         dst, recv = w_half(tp, half)
-        send(w_hbm.at[pl.ds(half * 128, 128)], dst, recv, (sp, tp_of(0, True)))
+        send("w", w_hbm.at[pl.ds(half * 128, 128)], dst, recv, (sp, tp_of(0, True)))
 
     def w_event(dy, half, links):
         ref, recv = w_half(tp_of(dy), half)
         arrived(ref, recv)
         for link in links:
             dev = tp_of(0, True) if link == 0 else tp_of(link)
-            send(ref, ref, recv, (sp, dev))
+            send("w", ref, ref, recv, (sp, dev))
 
     scale2 = HEAD_WIDTH ** (-0.5) * LOG2E
 
@@ -263,7 +265,7 @@
     att_in[tp] = att[pl.ds(tp * 32, 32), :]
     for dy, other in ((0, True), (1, False), (1, True), (3, False), (3, True), (2, False), (2, True)):
         to = tp_of(dy, other)
-        send(att.at[pl.ds(to * 32, 32)], att_in.at[tp], recv_att.at[tp], (sp, to))
+        send("att", att.at[pl.ds(to * 32, 32)], att_in.at[tp], recv_att.at[tp], (sp, to))
 
     for name in ("routing", "scores"):
         loads[name].wait()
@@ -327,11 +329,17 @@
         .reshape(EXPERTS, 16, 512)
     )
     rows_in[tp, 0, x] = slots[sp]
-    for g, dz in enumerate(BACK):
+    for dx in (0, 1, -1, 2):
+        to = sp_of(0, -dx)
+        for n, dy in ((0, 1), (1, -1)):
+            send("rows", slots.at[to], rows_in.at[tp, 0, x], recv_y.at[n, 0], (to, tp_of(dy)))
+        if dx != 0:
+            send("slots", slots.at[to], rows_in.at[tp, 0, x], recv_own.at[0], (to, tp))
+    for dz in AHEAD[1:]:
         for dx in (0, 1, -1, 2):
-            if (dz, dx) != (0, 0):
-                to = sp_of(-dz, -dx)
-                send(slots.at[to], rows_in.at[tp, g, x], recv_x.at[tp, g], (to, tp))
+            to = sp_of(-dz, -dx)
+            g = BACK.index(dz)
+            send("slots", slots.at[to], rows_in.at[tp, g, x], recv_own.at[g], (to, tp))
 
     out_no, in_no = iota((128, 128), 0), iota((128, 128), 1)
     sort = (
@@ -342,44 +350,38 @@
         in_no == (out_no % 32 // 4) * 16 + (out_no // 32) * 4 + out_no % 4
     ).astype(jnp.bfloat16)
 
-    def group_of(owner, g):
-        return rows_in.at[owner, g], recv_x.at[owner, g]
-
-    def spread_rows(owner, g, links):
-        ref, recv = group_of(owner, g)
-        for link in links:
-            dev = tp_of(0, True) if link == 0 else tp_of(link)
-            send(ref, ref, recv, (sp, dev))
+    def spread_rows(owner, g, to_far=None):
+        ref = rows_in.at[owner, g]
+        if to_far is not None:
+            send("rows", ref, ref, recv_y.at[2, g], (sp, tp_of(to_far)))
+        send("rows", ref, ref, recv_other.at[g // 2], (sp, tp_of(0, True)))
 
     def own(g):
-        ref, recv = group_of(tp, g)
-        arrived(rows_in.at[tp, g, pl.ds(0, 3)] if g == 0 else ref, recv)
-        spread_rows(tp, g, (1, -1, 0))
+        ref = rows_in.at[tp, g]
+        arrived(rows_in.at[tp, 0, pl.ds(0, 3)] if g == 0 else ref, recv_own.at[g])
+        if g != 0:
+            for n, dy in ((0, 1), (1, -1)):
+                send("rows", ref, ref, recv_y.at[n, g], (sp, tp_of(dy)))
+        spread_rows(tp, g)
 
     def near(g, dy):
         owner = tp_of(dy)
-        arrived(*group_of(owner, g))
-        spread_rows(owner, g, ((-dy, 0) if (g % 2 == 0) == (dy == -1) else (0,)))
+        arrived(rows_in.at[owner, g], recv_y.at[(1 + dy) // 2, g])
+        spread_rows(owner, g, -dy if (g % 2 == 0) == (dy == -1) else None)
 
     def far(g):
         owner = tp_of(2)
-        arrived(*group_of(owner, g))
-        spread_rows(owner, g, (0,))
+        arrived(rows_in.at[owner, g], recv_y.at[2, g])
+        spread_rows(owner, g)
 
     def sort_rows(o):
-        for g in (2 * o, 2 * o + 1):
-            for dy in (0, -1, 1, 2):
-                arrived(*group_of(tp_of(dy, True), g))
-
-        def sorted_rows(t, carry):
-            block = rows_in[t, pl.ds(2 * o, 2)].reshape(128, 512)
+        arrived(rows_in.at[0], recv_other.at[o])
+
+        for t in range(N_TP):
+            block = rows_in[t, 2 * o : 2 * o + 2].reshape(128, 512)
             out = jnp.dot(sort, block, preferred_element_type=jnp.float32).astype(jnp.bfloat16)
-            at = pl.ds(pl.multiple_of(t * 32, 32), 32)
             for j in range(4):
-                xr[at, 512 * j : 512 * (j + 1)] = out[32 * j : 32 * (j + 1)]
-            return carry
-
-        lax.fori_loop(0, N_TP, sorted_rows, 0)
+                xr[32 * t : 32 * t + 32, 512 * j : 512 * (j + 1)] = out[32 * j : 32 * (j + 1)]
 
     def up(o, n):
         if (o, n) == (0, 0):
@@ -400,7 +402,7 @@
         for dy in (2, 1, -1, 0):
             home = (y + dy + NY) % NY
             send(
-                parts.at[o, tp_of(dy, True)], parts_in.at[o, home], recv_part.at[o, home],
+                "parts", parts.at[o, tp_of(dy, True)], parts_in.at[o, home], recv_part.at[o],
                 (sp, tp_of(0, True)),
             )
 
@@ -408,15 +410,15 @@
 
     def chip_sum(o, dy):
         home = (y + dy + NY) % NY
-        if (o, dy) not in from_partner:
-            arrived(parts_in.at[o, home], recv_part.at[o, home])
-            from_partner.add((o, dy))
+        if o not in from_partner:
+            arrived(parts_in.at[o], recv_part.at[o])
+            from_partner.add(o)
         return parts[o, tp_of(dy)].astype(jnp.float32) + parts_in[o, home].astype(jnp.float32)
 
     def reduce_far(o):
         near_out[o, 0] = chip_sum(o, 2).astype(jnp.bfloat16)
-        send(near_out.at[o, 0, pl.ds(0, 16)], far_in.at[o, 0], recv_far.at[o, 0], (sp, tp_of(1)))
-        send(near_out.at[o, 0, pl.ds(16, 16)], far_in.at[o, 1], recv_far.at[o, 1], (sp, tp_of(-1)))
+        send("far", near_out.at[o, 0, pl.ds(0, 16)], far_in.at[o, 0], recv_far.at[o, 0], (sp, tp_of(1)))
+        send("far", near_out.at[o, 0, pl.ds(16, 16)], far_in.at[o, 1], recv_far.at[o, 1], (sp, tp_of(-1)))
 
     def reduce_near(o, n):
         dy = (1, -1)[n]
@@ -428,7 +430,7 @@
             jnp.bfloat16
         )
         near_out[o, 1 + n, rest, :] = mine[rest].astype(jnp.bfloat16)
-        send(near_out.at[o, 1 + n], near_in.at[o, n], recv_near.at[o, n], (sp, tp_of(dy)))
+        send("near", near_out.at[o, 1 + n], near_in.at[o, n], recv_near.at[o, n], (sp, tp_of(dy)))
 
     def give_back(o):
         whole = chip_sum(o, 0)
@@ -449,7 +451,7 @@
             for dx in (0, 1, -1, 2):
                 if (dz, dx) != (0, 0):
                     to = sp_of(dz, dx)
-                    send(back.at[o, 4 * n + to % NX], returned.at[sp], recv_back, (to, tp))
+                    send("back", back.at[o, 4 * n + to % NX], returned.at[sp], recv_back, (to, tp))
 
     last_down = {}
     for kind, o, *n in EXPERT_STEPS:
@@ -472,8 +474,19 @@
     for j in range(4):
         cols = slice(512 * j, 512 * (j + 1))
         out_ref[:, cols] = (middle_ref[:, cols] + routed[32 * j : 32 * (j + 1)]).astype(jnp.bfloat16)
-    for copy in sent:
-        copy.wait_send()
+    for kind, ref in (
+        ("A", kv.at[pl.ds(0, N_SP - 1), pl.ds(0, ROWS_A)]),
+        ("B", kv.at[pl.ds(0, N_SP - 1), pl.ds(ROWS_A, SEQ - ROWS_A)]),
+        ("w", wfull.at[pl.ds(0, N_TP - 1)]),
+        ("att", att_in.at[pl.ds(0, N_TP - 1)]),
+        ("slots", slots.at[pl.ds(0, N_SP - 1)]),
+        ("rows", rows_in.at[pl.ds(0, N_TP - 1)]),
+        ("parts", parts.at[pl.ds(0, 2)]),
+        ("far", parts_in.at[0]),
+        ("near", parts_in.at[pl.ds(0, 2)]),
+        ("back", returned.at[pl.ds(0, N_SP - 1)]),
+    ):
+        all_sent(kind, ref)
 
 
 def local(
@@ -532,14 +545,16 @@
             pltpu.VMEM((4, 8, 16, 512), bf16),
             pltpu.VMEM((EXPERTS, 16, 512), bf16),
             pltpu.VMEM((32, 2048), f32),
-            dma((256,)),
+            dma((len(KINDS),)),
             dma((N_SP,)),
             dma((N_SP,)),
             dma((N_TP, 2)),
             dma((N_TP,)),
             dma((14,)),
-            dma((N_TP, 8)),
-            dma((4, NY)),
+            dma((8,)),
+            dma((3, 8)),
+            dma((4,)),
+            dma((4,)),
             dma((4, 2)),
             dma((4, 2)),
             dma,

time: 117 us -> 111 us (0.949); the launches traced: 117 us -> 109 us
  Pallas kernels: 115 us -> 107 us
    pallas_call x1, Pallas kernels: 115 us -> 107 us  [local(): pl.pallas_call(layer_kernel, out_shape=jax.ShapeDtypeStruct((32, 2048), b...]
where the time goes in v4:
time: 111 us; the launch traced here: 109 us
  Pallas kernels  107 us (96%)
  local copies, waits for them, and re-layouts  1.57 us (1%)
    pallas_call x1, Pallas kernels, local(): pl.pallas_call(layer_kernel, out_shape=jax.ShapeDtypeStruct((32, 2048), b...  107 us

profile of v4, /device:TPU:0, one launch (start us, length us, event | category | flops | bytes accessed | tf_op | source)
XLA Modules:
  0.0 109.0 jit_solution(9381388794750461345)
XLA Ops:
  0.0 107.4 %layer.1 = bf16[32,2048]{1,0:T(8,128)(2,1)} custom-call(bf16[256,256]{1,0:T(8,128)(2,1)} %q_hbm.1, bf16[256,128]{1,0:T(8,128)(2,1)} %k_hbm.1, bf16[256,128]{1,0:T(8,128)(2,1)} %v_hbm.1, f32[1,128]{1,0:T(1,128)} %bitcast.8, f32[1,128]{1,0:T(1,128)} %bitcast.9, f32[2,128,128]{2,1,0:T(8,128)} %constant.2.clone.table_hbm, bf16[256,2048]{1,0:T(8,128)(2,1)} %w_hbm.1, ...), custom_call_target="tpu_custom_call" | custom-call | tf_op jit(solution)/shard_map/layer/pallas_call | solution.py:510
  107.4 1.6 %copy.16 = bf16[32,2048]{1,0:T(8,128)(2,1)} copy(bf16[32,2048]{1,0:T(8,128)(2,1)} %layer.1) | data formatting | bytes 262144

commit v5 on v4

--- a/solution.py
+++ b/solution.py
@@ -33,17 +33,17 @@
     ('B', 2, 2), ('C', -3, 0), ('A', 4, 2), ('A', 4, 1), ('C', -3, 1), ('B', 4, 1), ('B', 4, -1),
     ('C', 2, 0), ('C', 2, 1), ('B', 3, 2), ('C', 3, 0), ('C', 3, 1), ('B', 4, 2), ('C', 4, 0), ('C',
     4, 1))
-EXPERT_STEPS = (('own', 0), ('own', 1), ('own', 3), ('near', 0, -1), ('near', 0, 1), ('near', 1, -1), ('near', 1,
-    1), ('own', 4), ('near', 3, -1), ('near', 3, 1), ('own', 2), ('far', 0), ('own', 5), ('far', 1),
-    ('near', 4, -1), ('near', 4, 1), ('near', 2, -1), ('own', 6), ('far', 3), ('near', 5, -1),
-    ('sort', 0), ('near', 2, 1), ('up', 0, 0), ('own', 7), ('far', 4), ('up', 0, 1), ('near', 5, 1),
-    ('down', 0, 0), ('far', 2), ('down', 0, 1), ('near', 6, 1), ('near', 6, -1), ('near', 7, 1),
-    ('near', 7, -1), ('far', 5), ('sort', 1), ('rfar', 0), ('up', 1, 0), ('far', 6), ('up', 1, 1),
-    ('far', 7), ('down', 1, 0), ('down', 1, 1), ('sort', 2), ('rnear', 0, 0), ('rnear', 0, 1), ('up',
-    2, 0), ('up', 2, 1), ('down', 2, 0), ('down', 2, 1), ('rfar', 1), ('sort', 3), ('up', 3, 0),
-    ('up', 3, 1), ('down', 3, 0), ('down', 3, 1), ('back', 0), ('rfar', 2), ('rnear', 1, 0), ('rnear',
-    1, 1), ('rfar', 3), ('rnear', 2, 0), ('rnear', 2, 1), ('back', 1), ('rnear', 3, 0), ('rnear', 3,
-    1), ('back', 2), ('back', 3))
+EXPERT_STEPS = (('near', 0, -1), ('near', 0, 1), ('own', 0), ('own', 1), ('own', 3), ('far', 0), ('near', 1, 1),
+    ('own', 4), ('near', 1, -1), ('near', 3, 1), ('own', 2), ('near', 3, -1), ('own', 5), ('far', 1),
+    ('near', 4, -1), ('near', 4, 1), ('near', 2, -1), ('sort', 0), ('up', 0, 0), ('own', 6), ('far',
+    3), ('up', 0, 1), ('near', 5, -1), ('down', 0, 0), ('near', 2, 1), ('down', 0, 1), ('far', 4),
+    ('own', 7), ('near', 5, 1), ('far', 2), ('near', 6, 1), ('near', 6, -1), ('rfar', 0), ('sort', 1),
+    ('near', 7, -1), ('near', 7, 1), ('up', 1, 0), ('up', 1, 1), ('far', 5), ('down', 1, 0), ('far',
+    6), ('down', 1, 1), ('rnear', 0, 1), ('rnear', 0, 0), ('sort', 2), ('up', 2, 0), ('far', 7),
+    ('up', 2, 1), ('down', 2, 0), ('rfar', 1), ('down', 2, 1), ('sort', 3), ('up', 3, 0), ('up', 3,
+    1), ('back', 0), ('down', 3, 0), ('down', 3, 1), ('rfar', 2), ('rnear', 1, 0), ('rnear', 1, 1),
+    ('rfar', 3), ('rnear', 2, 0), ('rnear', 2, 1), ('back', 1), ('rnear', 3, 0), ('rnear', 3, 1),
+    ('back', 2), ('back', 3))
 
 
 def rms_scale(values, norm_gain):
@@ -202,7 +202,7 @@
         return []
 
     def w_half(owner, half):
-        return wfull.at[owner, pl.ds(half * 128, 128)], recv_w.at[owner, half]
+        return wfull.at[owner, pl.ds(half * 64, 64)], recv_w.at[owner, half]
 
     for half, dz, dx, link in (
         ("B", 0, 0, "z+"), ("B", 0, 0, "z-"), ("A", 0, 0, "x+"), ("A", 0, 0, "x-"),
@@ -210,12 +210,13 @@
         ("A", 0, 0, "z-"),
     ):
         pass_on(half, dz, dx, link)
-    for half, dev in ((0, tp_of(1)), (1, tp_of(-1)), (1, tp_of(1)), (0, tp_of(-1))):
-        dst, recv = w_half(tp, half)
-        send("w", w_hbm.at[pl.ds(half * 128, 128)], dst, recv, (sp, dev))
-    for half in (0, 1):
-        dst, recv = w_half(tp, half)
-        send("w", w_hbm.at[pl.ds(half * 128, 128)], dst, recv, (sp, tp_of(0, True)))
+    for n in range(4):
+        for part, dev in ((n, tp_of(1)), ((n + 2) % 4, tp_of(-1))):
+            dst, recv = w_half(tp, part)
+            send("w", w_hbm.at[pl.ds(part * 64, 64)], dst, recv, (sp, dev))
+    for part in range(4):
+        dst, recv = w_half(tp, part)
+        send("w", w_hbm.at[pl.ds(part * 64, 64)], dst, recv, (sp, tp_of(0, True)))
 
     def w_event(dy, half, links):
         ref, recv = w_half(tp_of(dy), half)
@@ -246,7 +247,10 @@
             )
             m_ref[h] = m_new
 
-    w_plan = {30: ((-1, 0, (1, 0)), (1, 1, (-1, 0))), 70: ((-1, 1, (0,)), (1, 0, (0,)))}
+    w_plan = {
+        16: ((-1, 0, (1, 0)), (1, 2, (-1, 0))), 26: ((-1, 1, (1, 0)), (1, 3, (-1, 0))),
+        52: ((-1, 2, (0,)), (1, 0, (0,))), 71: ((-1, 3, (0,)), (1, 1, (0,))),
+    }
     for count, (half, dz, dx) in enumerate(ATTENTION_STEPS):
         if half == "C":
             attend((z - dz + NZ) % NZ, dx)
@@ -266,6 +270,9 @@
     for dy, other in ((0, True), (1, False), (1, True), (3, False), (3, True), (2, False), (2, True)):
         to = tp_of(dy, other)
         send("att", att.at[pl.ds(to * 32, 32)], att_in.at[tp], recv_att.at[tp], (sp, to))
+
+    w_event(2, 0, (0,))
+    w_event(2, 2, (0,))
 
     for name in ("routing", "scores"):
         loads[name].wait()
@@ -304,8 +311,8 @@
 
     for name in ("w", "x", "fg"):
         loads[name].wait()
-    w_event(2, 0, (0,))
     w_event(2, 1, (0,))
+    w_event(2, 3, (0,))
     total = jnp.zeros((32, 2048), jnp.float32)
     order = [(0, False), (1, False), (3, False), (2, False), (0, True), (1, True), (3, True), (2, True)]
     for dy, other in order:
@@ -313,7 +320,7 @@
         if (dy, other) != (0, False):
             arrived(att_in.at[owner], recv_att.at[owner])
         if other:
-            for half in (0, 1):
+            for half in range(4):
                 ref, recv = w_half(owner, half)
                 arrived(ref, recv)
         part = jnp.dot(att_in[owner], wfull[owner], preferred_element_type=jnp.float32)
@@ -548,7 +555,7 @@
             dma((len(KINDS),)),
             dma((N_SP,)),
             dma((N_SP,)),
-            dma((N_TP, 2)),
+            dma((N_TP, 4)),
             dma((N_TP,)),
             dma((14,)),
             dma((8,)),

time: 111 us -> 109 us (0.982)
    pallas_call x1, Pallas kernels: 107 us -> 106 us  [local(): pl.pallas_call(layer_kernel, out_shape=jax.ShapeDtypeStruct((32, 2048), b...]
where the time goes in v5:
time: 109 us; the launch traced here: 108 us
  Pallas kernels  106 us (97%)
  local copies, waits for them, and re-layouts  1.57 us (1%)
    pallas_call x1, Pallas kernels, local(): pl.pallas_call(layer_kernel, out_shape=jax.ShapeDtypeStruct((32, 2048), b...  106 us

profile of v5, /device:TPU:0, one launch (start us, length us, event | category | flops | bytes accessed | tf_op | source)
XLA Modules:
  0.0 107.6 jit_solution(3255424142591132803)
XLA Ops:
  0.0 106.0 %layer.1 = bf16[32,2048]{1,0:T(8,128)(2,1)} custom-call(bf16[256,256]{1,0:T(8,128)(2,1)} %q_hbm.1, bf16[256,128]{1,0:T(8,128)(2,1)} %k_hbm.1, bf16[256,128]{1,0:T(8,128)(2,1)} %v_hbm.1, f32[1,128]{1,0:T(1,128)} %bitcast.8, f32[1,128]{1,0:T(1,128)} %bitcast.9, f32[2,128,128]{2,1,0:T(8,128)} %constant.2.clone.table_hbm, bf16[256,2048]{1,0:T(8,128)(2,1)} %w_hbm.1, ...), custom_call_target="tpu_custom_call" | custom-call | tf_op jit(solution)/shard_map/layer/pallas_call | solution.py:517
  106.0 1.6 %copy.16 = bf16[32,2048]{1,0:T(8,128)(2,1)} copy(bf16[32,2048]{1,0:T(8,128)(2,1)} %layer.1) | data formatting | bytes 262144
